TPU v7x, 512 devices: a whole 4x8x8 slice. The times are simulated.
512 devices in a mesh: sp: 32 (over z, x), tp: 16 (over y, core).
Axes of the slice: x: 4, y: 8, z: 8, core: 2. Of those that a mesh axis runs over, the one named last changes fastest.
Arguments:
- queries: bfloat16 [4096, 2048], P('sp', 'tp'), may hold values from -440 to 440
- key_rows: bfloat16 [4096, 1024], P('sp', 'tp'), may hold values from -6 to 6
- value_rows: bfloat16 [4096, 1024], P('sp', 'tp'), may hold values from -6 to 6
- sink_logits: float32 [32], P('tp'), may hold values from -6 to 6
- out_weight: bfloat16 [2048, 2048], P('tp'), may hold values from -0.125 to 0.125
- residual: bfloat16 [4096, 2048], P('sp'), may hold values from -3 to 3
- norm_gain: float32 [2048], replicated, may hold values from 0.1 to 1.9
- routes: int32 [4096, 2], P('sp'), may hold values from 0 to 31, all different within a row; in each aligned block of 128 rows (0 to 127, 128 to 255, ...) at most 16 rows name the same one
- route_weights: float32 [4096, 2], P('sp'), may hold values from 0.2 to 1
- gate_weight: bfloat16 [32, 2048, 4096], P('sp', None, 'tp'), may hold values from -0.125 to 0.125
- up_weight: bfloat16 [32, 2048, 4096], P('sp', None, 'tp'), may hold values from -0.125 to 0.125
- down_weight: bfloat16 [32, 4096, 2048], P('sp', 'tp'), may hold values from -0.09375 to 0.09375
Outputs:
- layer_out: bfloat16 [4096, 2048], P('sp')
Inputs may be any that keep to these rules, and one draw needn't show every extreme that they name: `routes`: each row names 2 different experts. In each aligned block of 128 rows (the rows of one index of sp) no expert is named by more than 16 rows, a bound that some block reaches.
All inputs are finite; a program needn't handle non-finite values.
Results may differ from a plain program's by a relative error of at most 0.02.
Values may be sent and summed in bfloat16 or wider, within the bound.
A program may use at most 64 MiB of HBM per device.

v0:
```python
import jax
import jax.numpy as jnp
from jax import lax
from jax.sharding import Mesh
from jax.sharding import PartitionSpec as P

HEAD_DIM = 64
QH = 32
WINDOW = 128
TOP = 2
TP = ("tp_0", "tp_1")


def from_behind(array, axis, by):
    peers = lax.axis_size(axis)
    pairs = [(i, i + by) for i in range(peers) if 0 <= i + by < peers]
    return lax.ppermute(array, axis, pairs)


def split_up(array, dim, peers):
    dims = array.shape
    pieces = array.reshape(*dims[:dim], peers, dims[dim] // peers, *dims[dim + 1 :])
    return jnp.moveaxis(pieces, dim, 0)


def summed_on_arrival(array, axis, dim):
    pieces = split_up(array, dim, lax.axis_size(axis))
    arrived = lax.all_to_all(pieces, axis, split_axis=0, concat_axis=0, tiled=True)
    return arrived.astype(jnp.float32).sum(axis=0)


def sum_by_axis(array, axes, dim):
    far, near = axes
    own = summed_on_arrival(split_up(array, dim, lax.axis_size(far)), near, dim + 1)
    return jnp.sum(
        lax.all_to_all(own.astype(jnp.bfloat16), far, 0, 0, tiled=True).astype(jnp.float32), axis=0
    )


def rows_for(lines, peers):
    spare = -len(lines) % peers
    return jnp.pad(lines, [(0, spare)] + [(0, 0)] * (lines.ndim - 1))


def from_everyone(array, axis):
    copies = jnp.broadcast_to(array, (lax.axis_size(axis), *array.shape))
    return lax.all_to_all(copies, axis, split_axis=0, concat_axis=0, tiled=True)


def laid_out(pieces, dim):
    dims = list(pieces.shape[1:])
    dims[dim] *= pieces.shape[0]
    return jnp.moveaxis(pieces, 0, dim).reshape(dims)


def gathered_by_axis(array, axes, dim):
    far, near = axes
    pieces = from_everyone(from_everyone(array, far), near)
    return laid_out(pieces.swapaxes(0, 1).reshape(-1, *array.shape), dim)


def sum_by_parts(array, axes):
    lines = array.reshape(-1, array.shape[-1])
    own = sum_by_axis(rows_for(lines, lax.axis_size(axes[0]) * lax.axis_size(axes[1])), axes, 0)
    whole = gathered_by_axis(own.astype(jnp.bfloat16), axes, 0)
    return whole[: len(lines)].reshape(array.shape).astype(jnp.float32)


def per_device(
    queries,
    key_rows,
    value_rows,
    sink_logits,
    out_weight,
    residual,
    norm_gain,
    routes,
    route_weights,
    gate_weight,
    up_weight,
    down_weight,
):
    rows_here = queries.shape[0]
    width = residual.shape[1]
    heads_here = queries.shape[1] // HEAD_DIM
    kv_here = key_rows.shape[1] // HEAD_DIM
    group_size = heads_here // kv_here
    blocks = rows_here // WINDOW
    rim_rows = jnp.stack([key_rows, value_rows])
    before = from_behind(rim_rows, "sp", 1)
    key_ext = jnp.concatenate([before[0], key_rows], axis=0).reshape(
        blocks + 1, WINDOW, kv_here, HEAD_DIM
    )
    val_ext = jnp.concatenate([before[1], value_rows], axis=0).reshape(
        blocks + 1, WINDOW, kv_here, HEAD_DIM
    )
    key_pair = jnp.concatenate([key_ext[:-1], key_ext[1:]], axis=1)
    val_pair = jnp.concatenate([val_ext[:-1], val_ext[1:]], axis=1)
    query_blocks = queries.reshape(blocks, WINDOW, kv_here, group_size, HEAD_DIM)
    scores = jnp.einsum(
        "bqkgd,bckd->bkgqc", query_blocks, key_pair, preferred_element_type=jnp.float32
    ) * HEAD_DIM ** (-0.5)
    distance = jnp.arange(WINDOW)[:, None] + WINDOW - jnp.arange(2 * WINDOW)[None, :]
    offset = lax.axis_index("sp") * rows_here
    key_global = (
        offset
        + jnp.arange(blocks)[:, None, None] * WINDOW
        + jnp.arange(2 * WINDOW)[None, None, :]
        - WINDOW
    )
    allowed = (distance >= 0)[None] & (distance <= WINDOW)[None] & (key_global >= 0)
    head_ids = lax.axis_index(TP) * heads_here + jnp.arange(heads_here)
    slopes = jnp.exp2(-8.0 * (head_ids + 1).astype(jnp.float32) / QH).reshape(kv_here, group_size)
    scores = scores - slopes[None, :, :, None, None] * distance.astype(jnp.float32)
    scores = jnp.where(allowed[:, None, None], scores, -jnp.inf)
    row_peak = jnp.max(scores, axis=-1, keepdims=True)
    log_total = row_peak + jnp.log(jnp.sum(jnp.exp(scores - row_peak), axis=-1, keepdims=True))
    weights_bf = jnp.exp(scores - log_total).astype(jnp.bfloat16)
    attended = jnp.einsum(
        "bkgqc,bckd->bqkgd", weights_bf, val_pair, preferred_element_type=jnp.float32
    )
    keep_factor = jax.nn.sigmoid(
        log_total[..., 0] - sink_logits.reshape(kv_here, group_size)[None, :, :, None]
    )
    keep_factor = jnp.transpose(keep_factor, (0, 3, 1, 2))[..., None]
    attended = (
        (attended * keep_factor).astype(jnp.bfloat16).reshape(rows_here, heads_here * HEAD_DIM)
    )
    partial_value = jnp.dot(attended, out_weight, preferred_element_type=jnp.float32)
    partial_value = lax.optimization_barrier(partial_value.astype(jnp.bfloat16)).astype(jnp.float32)
    head_total = sum_by_parts(partial_value.astype(jnp.bfloat16), ("tp_0", "tp_1"))
    mixed_state = (residual.astype(jnp.float32) + head_total).astype(jnp.bfloat16)
    state32 = mixed_state.astype(jnp.float32)
    normed = (
        state32 * lax.rsqrt(jnp.mean(state32 * state32, axis=-1, keepdims=True) + 1e-06) * norm_gain
    ).astype(jnp.bfloat16)
    experts = lax.axis_size("sp")
    capacity = 2 * rows_here * TOP // experts
    flat_routes = routes.reshape(-1)
    member = (flat_routes[:, None] == jnp.arange(experts)[None, :]).astype(jnp.int32)
    slot_rank = jnp.sum((jnp.cumsum(member, axis=0) - 1) * member, axis=1)
    slot_index = flat_routes * capacity + slot_rank
    picker = (jnp.arange(experts * capacity)[:, None] == slot_index[None, :]).astype(jnp.int32)
    picker = jnp.sum(picker.reshape(experts * capacity, rows_here, TOP), axis=-1).astype(
        jnp.bfloat16
    )
    outgoing = (
        jnp.dot(picker, normed, preferred_element_type=jnp.float32)
        .astype(jnp.bfloat16)
        .reshape(experts, capacity, width)
    )
    w_gate = gate_weight[0]
    w_up = up_weight[0]
    w_down = down_weight[0]
    slot_share = capacity // lax.axis_size(TP)
    mine = lax.dynamic_slice_in_dim(outgoing, lax.axis_index(TP) * slot_share, slot_share, 1)
    arrived = lax.all_to_all(mine, "sp", split_axis=0, concat_axis=0, tiled=True)
    gathered = gathered_by_axis(arrived, ("tp_0", "tp_1"), 1)
    flat_rows = gathered.reshape(-1, width)
    gate_pre = jnp.dot(flat_rows, w_gate, preferred_element_type=jnp.float32)
    up_pre = jnp.dot(flat_rows, w_up, preferred_element_type=jnp.float32)
    activated = (jax.nn.silu(gate_pre) * up_pre).astype(jnp.bfloat16)
    result = jnp.dot(activated, w_down, preferred_element_type=jnp.float32)
    result = lax.optimization_barrier(result.astype(jnp.bfloat16)).astype(jnp.float32)
    summed = summed_on_arrival(result.reshape(gathered.shape).astype(jnp.bfloat16), TP, 1).astype(
        jnp.bfloat16
    )
    back_rows = lax.all_to_all(summed, "sp", split_axis=0, concat_axis=0, tiled=True)
    returned = gathered_by_axis(back_rows, ("tp_0", "tp_1"), 1)
    slot_table = returned.reshape(experts * capacity, width)
    picked = jnp.take(slot_table, slot_index, axis=0).reshape(rows_here, TOP, width)
    expert_mix = jnp.sum(route_weights[..., None] * picked.astype(jnp.float32), axis=1)
    return (state32 + expert_mix).astype(jnp.bfloat16)


def solution(mesh):
    torus = Mesh(mesh.devices.reshape(mesh.shape["sp"], 8, 2), ("sp", "tp_0", "tp_1"))
    placed = (
        P("sp", TP),
        P("sp", TP),
        P("sp", TP),
        P(TP),
        P(TP, None),
        P("sp", None),
        P(),
        P("sp", None),
        P("sp", None),
        P("sp", None, TP),
        P("sp", None, TP),
        P("sp", TP, None),
    )
    return jax.shard_map(
        per_device, mesh=torus, in_specs=placed, out_specs=P("sp", None), check_vma=False
    )
```

profile of v0, /device:TPU:1, one launch (start us, length us, event | category | flops | bytes accessed | tf_op | source)
XLA Modules:
  0.0 252.0 jit_solution(2691654615877382855)
XLA Ops:
  0.0 0.8 pad_maximum_fusion
  0.8 3.9 %collective-permute-start = (bf16[2,128,64]{1,2,0:T(8,128)(2,1)S(1)}, bf16[2,128,64]{1,2,0:T(8,128)(2,1)S(1)}, u32[]{:S(2)}, u32[]{:S(2)}) collective-permute-start(bf16[2,128,64]{1,2,0:T(8,128)(2,1)S(1)} %pad_maximum_fusion), channel_id=1, source_target_pairs={{0,16},{16,32},{32,48},{48,64},{64,80},{80,96},{96,112},{112,128},... | collective-permute-start | bytes 98312 | tf_op jit(solution)/shard_map/ppermute | solution.py:17
  4.9 0.9 copy.72
  5.8 1.0 fusion.52
  6.9 0.7 fusion.45
  7.6 0.9 fusion.5
  8.5 1.4 convolution_convert_fusion.2
  9.9 8.5 %all_to_all.67 = bf16[2,8,8,2048]{3,2,1,0:T(8,128)(2,1)S(1)} all-to-all(bf16[2,8,8,2048]{3,2,1,0:T(8,128)(2,1)S(1)} %bitcast.137), channel_id=1, replica_groups=mesh['sp'=32,'tp_0'=8,'tp_1'=2] {'tp_1'}, dimensions={0} | all-to-all | bytes 1048576 | tf_op jit(solution)/shard_map/all_to_all | solution.py:28
  18.4 0.8 reduce_sum.88
  19.2 3.6 %all-to-all-start.1 = ((bf16[8,8,2048]{2,1,0:T(8,128)(2,1)}), bf16[8,8,2048]{2,1,0:T(8,128)(2,1)S(1)}, u32[]{:S(2)}, u32[]{:S(2)}) async-start(bf16[8,8,2048]{2,1,0:T(8,128)(2,1)} %reduce_sum.88), calls=%async_computation.1 | async-start | bytes 524288 | tf_op jit(solution)/shard_map/all_to_all | solution.py:36
  23.1 0.6 reduce-window.6
  23.7 10.2 %all-to-all-done.1 = bf16[8,8,2048]{2,1,0:T(8,128)(2,1)S(1)} async-done(((bf16[8,8,2048]{2,1,0:T(8,128)(2,1)}), bf16[8,8,2048]{2,1,0:T(8,128)(2,1)S(1)}, u32[]{:S(2)}, u32[]{:S(2)}) %all-to-all-start.1) | async-done | bytes 262176 | tf_op jit(solution)/shard_map/all_to_all | solution.py:36
  34.0 0.7 broadcast_in_dim.58
  34.7 3.4 %all-to-all-start.2 = ((bf16[8,8,2048]{2,1,0:T(8,128)(2,1)}), bf16[8,8,2048]{2,1,0:T(8,128)(2,1)S(1)}, u32[]{:S(2)}, u32[]{:S(2)}) async-start(bf16[8,8,2048]{2,1,0:T(8,128)(2,1)} %broadcast_in_dim.58), calls=%async_computation.2 | async-start | bytes 524288 | tf_op jit(solution)/shard_map/all_to_all | solution.py:47
  38.1 0.2 slice_reduce_fusion
  38.9 8.9 %all-to-all-done.2 = bf16[8,8,2048]{2,1,0:T(8,128)(2,1)S(1)} async-done(((bf16[8,8,2048]{2,1,0:T(8,128)(2,1)}), bf16[8,8,2048]{2,1,0:T(8,128)(2,1)S(1)}, u32[]{:S(2)}, u32[]{:S(2)}) %all-to-all-start.2) | async-done | bytes 262176 | tf_op jit(solution)/shard_map/all_to_all | solution.py:47
  47.8 6.8 %all_to_all.68 = bf16[2,8,8,2048]{3,2,1,0:T(8,128)(2,1)S(1)} all-to-all(bf16[2,8,8,2048]{3,2,1,0:T(8,128)(2,1)S(1)} %broadcast_in_dim.59), channel_id=1, replica_groups=mesh['sp'=32,'tp_0'=8,'tp_1'=2] {'tp_1'}, dimensions={0} | all-to-all | bytes 1048576 | tf_op jit(solution)/shard_map/all_to_all | solution.py:47
  54.8 0.3 fusion.6
  55.1 0.8 copy-done.1
  55.9 0.8 convolution_convert_fusion.1
  56.6 0.3 constant_dynamic-slice_fusion
  56.9 0.5 broadcast.269
  57.5 1.4 reduce.8
  58.9 23.7 %all_to_all.69 = bf16[32,2,1024]{2,1,0:T(2,128)(2,1)S(1)} all-to-all(bf16[32,2,1024]{2,1,0:T(2,128)(2,1)S(1)} %reshape.355), channel_id=1, replica_groups=mesh['sp'=32,'tp_0'=8,'tp_1'=2] {'sp'}, dimensions={0} | all-to-all | bytes 262144 | tf_op jit(solution)/shard_map/all_to_all | solution.py:157
  82.9 28.3 %all_to_all.70 = bf16[8,32,1,2048]{3,1,2,0:T(8,128)(2,1)S(1)} all-to-all(bf16[8,32,1,2048]{3,1,2,0:T(8,128)(2,1)S(1)} %broadcast_in_dim.61), channel_id=1, replica_groups=mesh['sp'=32,'tp_0'=8,'tp_1'=2] {'tp_0'}, dimensions={0} | all-to-all | bytes 2097152 | tf_op jit(solution)/shard_map/all_to_all | solution.py:47
  111.2 0.3 broadcast_in_dim.62
  111.5 8.8 %all_to_all.71 = bf16[2,8,32,1,2048]{4,2,1,3,0:T(8,128)(2,1)S(1)} all-to-all(bf16[2,8,32,1,2048]{4,2,1,3,0:T(8,128)(2,1)S(1)} %broadcast_in_dim.62), channel_id=1, replica_groups=mesh['sp'=32,'tp_0'=8,'tp_1'=2] {'tp_1'}, dimensions={0} | all-to-all | bytes 4194304 | tf_op jit(solution)/shard_map/all_to_all | solution.py:47
  120.3 0.2 copy.82
  120.6 1.2 copy.83
  121.8 1.5 fusion.14
  123.3 5.0 %convolution_convert_fusion = bf16[512,2048]{1,0:T(8,128)(2,1)} fusion(bf16[512,2048]{1,0:T(8,128)(2,1)S(1)} %bitcast.134, bf16[1,256,2048]{2,1,0:T(8,128)(2,1)S(1)} %copy-done, bf16[1,2048,256]{2,1,0:T(8,128)(2,1)} %param.22, f32[512,256]{1,0:T(8,128)} %fusion.14), kind=kOutput, calls=%fused_computation.1 | convolution fusion | flops 1075576832 | bytes 6815744 | tf_op jit(solution)/shard_map/dot_general | solution.py:163
  128.3 2.7 %copy.100 = bf16[32,16,1,2048]{3,0,2,1:T(8,128)(2,1)S(1)} copy(bf16[32,16,1,2048]{3,1,0,2:T(8,128)(2,1)} %bitcast.135) | data formatting | bytes 4194304 | tf_op jit(solution)/shard_map/convert_element_type | solution.py:165
  131.1 53.8 %all_to_all.72 = bf16[16,32,1,2048]{3,1,2,0:T(8,128)(2,1)S(1)} all-to-all(bf16[16,32,1,2048]{3,1,2,0:T(8,128)(2,1)S(1)} %bitcast.128), channel_id=1, replica_groups=mesh['sp'=32,'tp_0'=8,'tp_1'=2] {'tp_0','tp_1'}, dimensions={0} | all-to-all | bytes 4194304 | tf_op jit(solution)/shard_map/all_to_all | solution.py:28
  184.9 0.4 reduce_sum.94
  185.3 0.6 reduce.9
  186.0 14.0 %all_to_all.73 = bf16[32,2,1024]{2,1,0:T(2,128)(2,1)S(1)} all-to-all(bf16[32,2,1024]{2,1,0:T(2,128)(2,1)S(1)} %reshape.357), channel_id=1, replica_groups=mesh['sp'=32,'tp_0'=8,'tp_1'=2] {'sp'}, dimensions={0} | all-to-all | bytes 262144 | tf_op jit(solution)/shard_map/all_to_all | solution.py:168
  200.3 1.1 broadcast_in_dim.63
  201.4 3.6 %all-to-all-start.9 = ((bf16[8,32,1,2048]{3,1,2,0:T(8,128)(2,1)}), bf16[8,32,1,2048]{3,1,2,0:T(8,128)(2,1)S(1)}, u32[]{:S(2)}, u32[]{:S(2)}) async-start(bf16[8,32,1,2048]{3,1,2,0:T(8,128)(2,1)} %broadcast_in_dim.63), calls=%async_computation.9 | async-start | bytes 2097152 | tf_op jit(solution)/shard_map/all_to_all | solution.py:47
  205.5 28.6 %all-to-all-done.9 = bf16[8,32,1,2048]{3,1,2,0:T(8,128)(2,1)S(1)} async-done(((bf16[8,32,1,2048]{3,1,2,0:T(8,128)(2,1)}), bf16[8,32,1,2048]{3,1,2,0:T(8,128)(2,1)S(1)}, u32[]{:S(2)}, u32[]{:S(2)}) %all-to-all-start.9) | async-done | bytes 1048608 | tf_op jit(solution)/shard_map/all_to_all | solution.py:47
  234.1 0.6 copy.86
  234.7 0.3 broadcast_in_dim.64
  235.0 5.5 %all_to_all.74 = bf16[2,8,32,1,2048]{4,1,2,3,0:T(8,128)(2,1)S(1)} all-to-all(bf16[2,8,32,1,2048]{4,1,2,3,0:T(8,128)(2,1)S(1)} %broadcast_in_dim.64), channel_id=1, replica_groups=mesh['sp'=32,'tp_0'=8,'tp_1'=2] {'tp_1'}, dimensions={0} | all-to-all | bytes 4194304 | tf_op jit(solution)/shard_map/all_to_all | solution.py:47
  240.5 1.2 copy.87
  241.6 1.2 copy.88
  242.8 2.3 gather_fusion
  245.1 1.8 gather.7
  246.9 4.1 %multiply_reduce_fusion = f32[128,2048]{1,0:T(8,128)S(1)} fusion(bf16[128,2,2048]{2,1,0:T(2,128)(2,1)S(1)} %gather.7, pred[128,2]{1,0:T(8,128)(4,1)S(1)} %copy.81, f32[128,2]{1,0:T(8,128)S(1)} %copy.76), kind=kLoop, calls=%fused_computation.5 | loop fusion | flops 1835008 | bytes 2098432 | tf_op jit(solution)/shard_map/reduce_sum | solution.py:172
  251.0 0.9 fusion.9
  (53 shorter events, 2.5 us)
Async XLA Ops:
  0.0 123.3 %copy-start = (bf16[1,256,2048]{2,1,0:T(8,128)(2,1)S(1)}, bf16[1,256,2048]{2,1,0:T(8,128)(2,1)}, u32[]{:S(2)}) copy-start(bf16[1,256,2048]{2,1,0:T(8,128)(2,1)} %param.23) | copy-start | bytes 3145732
  0.8 5.0 %collective-permute-start = (bf16[2,128,64]{1,2,0:T(8,128)(2,1)S(1)}, bf16[2,128,64]{1,2,0:T(8,128)(2,1)S(1)}, u32[]{:S(2)}, u32[]{:S(2)}) collective-permute-start(bf16[2,128,64]{1,2,0:T(8,128)(2,1)S(1)} %pad_maximum_fusion), channel_id=1, source_target_pairs={{0,16},{16,32},{32,48},{48,64},{64,80},{80,96},{96,112},{112,128},... | collective-permute-start | bytes 98312 | tf_op jit(solution)/shard_map/ppermute | solution.py:17
  8.5 14.3 %copy-start.4 = (s32[128,2]{0,1:T(2,128)S(1)}, s32[128,2]{0,1:T(2,128)}, u32[]{:S(2)}) copy-start(s32[128,2]{0,1:T(2,128)} %param.19) | copy-start | bytes 3076
  19.2 14.7 %all-to-all-start.1 = ((bf16[8,8,2048]{2,1,0:T(8,128)(2,1)}), bf16[8,8,2048]{2,1,0:T(8,128)(2,1)S(1)}, u32[]{:S(2)}, u32[]{:S(2)}) async-start(bf16[8,8,2048]{2,1,0:T(8,128)(2,1)} %reduce_sum.88), calls=%async_computation.1 | async-start | bytes 524288 | tf_op jit(solution)/shard_map/all_to_all | solution.py:36
  34.7 13.1 %all-to-all-start.2 = ((bf16[8,8,2048]{2,1,0:T(8,128)(2,1)}), bf16[8,8,2048]{2,1,0:T(8,128)(2,1)S(1)}, u32[]{:S(2)}, u32[]{:S(2)}) async-start(bf16[8,8,2048]{2,1,0:T(8,128)(2,1)} %broadcast_in_dim.58), calls=%async_computation.2 | async-start | bytes 524288 | tf_op jit(solution)/shard_map/all_to_all | solution.py:47
  38.1 16.7 %copy-start.3 = (bf16[128,2048]{1,0:T(8,128)(2,1)S(1)}, bf16[128,2048]{1,0:T(8,128)(2,1)}, u32[]{:S(2)}) copy-start(bf16[128,2048]{1,0:T(8,128)(2,1)} %param.17) | copy-start | bytes 1572868
  54.7 1.2 copy-start.5
  55.0 0.8 copy-start.1
  120.6 1.2 copy-start.7
  200.1 5.3 %copy-start.6 = (f32[128,2]{0,1:T(2,128)S(1)}, f32[128,2]{0,1:T(2,128)}, u32[]{:S(2)}) copy-start(f32[128,2]{0,1:T(2,128)} %param.20) | copy-start | bytes 3076
  201.4 32.8 %all-to-all-start.9 = ((bf16[8,32,1,2048]{3,1,2,0:T(8,128)(2,1)}), bf16[8,32,1,2048]{3,1,2,0:T(8,128)(2,1)S(1)}, u32[]{:S(2)}, u32[]{:S(2)}) async-start(bf16[8,32,1,2048]{3,1,2,0:T(8,128)(2,1)} %broadcast_in_dim.63), calls=%async_computation.9 | async-start | bytes 2097152 | tf_op jit(solution)/shard_map/all_to_all | solution.py:47
  245.1 5.9 %copy-start.2 = (bf16[128,2048]{1,0:T(8,128)(2,1)S(1)}, bf16[128,2048]{1,0:T(8,128)(2,1)}, u32[]{:S(2)}) copy-start(bf16[128,2048]{1,0:T(8,128)(2,1)} %copy-done.1) | copy-start | bytes 1572868
where the time goes:
time: 253 us; the launch traced here: 252 us
  blocking collectives  150 us (59%)
  waiting for transfers between devices  47.8 us (19%)
  local copies, waits for them, and re-layouts  18.1 us (7%)
  starting transfers between devices  14.5 us (6%)
  other arithmetic  11.2 us (4%)
  matrix products  10.5 us (4%)
    all_to_all x2, blocking collectives, summed_on_arrival(): lax.all_to_all(pieces, axis, split_axis=0, concat_axis=0, tiled=True)  62.3 us
    all_to_all x4, blocking collectives, from_everyone(): return lax.all_to_all(copies, axis, split_axis=0, concat_axis=0, tiled=True)  49.5 us
    all_to_all x2, waiting for transfers between devices, from_everyone(): return lax.all_to_all(copies, axis, split_axis=0, concat_axis=0, tiled=True)  37.5 us
    all_to_all x1, blocking collectives, per_device(): lax.all_to_all(mine, 'sp', split_axis=0, concat_axis=0, tiled=True)  23.7 us
    all_to_all x1, blocking collectives, per_device(): lax.all_to_all(summed, 'sp', split_axis=0, concat_axis=0, tiled=True)  14 us
    all_to_all x1, waiting for transfers between devices, sum_by_axis(): lax.all_to_all(own.astype(jnp.bfloat16), far, 0, 0, tiled=True)  10.2 us
    all_to_all x2, starting transfers between devices, from_everyone(): return lax.all_to_all(copies, axis, split_axis=0, concat_axis=0, tiled=True)  6.97 us
  transfers between devices with their start and end apart: 4, of which 3 were waited for; matrix products, arithmetic and copies ran while one was open for 1% of the time, Pallas kernels for 0%

commit v1 on v0

v1 whole, which is shorter than its diff:
```python
import functools

import jax
import jax.numpy as jnp
from jax import lax
from jax.experimental import pallas as pl
from jax.experimental.pallas import tpu as pltpu
from jax.sharding import Mesh
from jax.sharding import PartitionSpec as P

HEAD_DIM = 64
QH = 32
TOP = 2
T = 128
L = 128
G = 4
BF = jnp.bfloat16
F32 = jnp.float32
NX = 4


def dot(a, b, dims=((1,), (0,))):
    return lax.dot_general(a, b, (dims, ((), ())), preferred_element_type=F32)


def offsets(nz, nx):
    def far(k):
        dz, dx = k // nx, k % nx
        return min(dz, nz - dz) + min(dx, nx - dx)

    return [(k // nx, k % nx) for k in sorted(range(nz * nx), key=lambda k: (far(k), k))]


def layer(
    dims,
    q_ref,
    k_ref,
    v_ref,
    sink_ref,
    wo_hbm,
    res_hbm,
    gain_ref,
    routes_ref,
    rw_ref,
    wg_hbm,
    wu_hbm,
    wd_hbm,
    out_hbm,
    wo,
    wg,
    wu,
    wd,
    res,
    halo,
    p0_ref,
    p1_ref,
    pick_ref,
    own1,
    ps1,
    pr1,
    r1s,
    r1r,
    state_ref,
    disp,
    ag,
    acc_g,
    acc_u,
    ssq,
    act_ref,
    own2,
    ps2,
    pr2,
    r2s,
    r2r,
    out2,
    ret,
    fin,
    loc_sem,
    send_sem,
    halo_sem,
    p1_sem,
    r1_sem,
    disp_sem,
    agr_sem,
    agd_sem,
    p2_sem,
    r2_sem,
    ret_sem,
    fin_sem,
    find_sem,
):
    nz, nx, ny = dims
    ns = nz * nx
    slots = ns * disp.shape[1]
    cap = disp.shape[1]
    half = ny // 2
    per = ns // G
    rows = slots // G
    z, x, y, c = (lax.axis_index(a) for a in ("z", "x", "y", "c"))
    me_s = z * nx + x
    me_j = 2 * y + c
    pos = offsets(nz, nx)

    def at_y(rel):
        return lax.rem(y + (rel + ny) % ny, ny)

    def sp_at(dz, dx):
        return lax.rem(z + dz % nz, nz), lax.rem(x + dx % nx, nx)

    partner = (z, x, y, 1 - c)

    def remote(src, dst, s, r, dev):
        cp = pltpu.make_async_remote_copy(
            src_ref=src,
            dst_ref=dst,
            send_sem=s,
            recv_sem=r,
            device_id=dev,
            device_id_type=pl.DeviceIdType.MESH,
        )
        cp.start()

    def take(ref, sem):
        pltpu.make_async_copy(ref, ref, sem).wait()

    barrier = pltpu.get_barrier_semaphore()
    for dz, dx in pos[1:]:
        tz, tx = sp_at(dz, dx)
        pl.semaphore_signal(
            barrier, inc=1, device_id=(tz, tx, y, c), device_id_type=pl.DeviceIdType.MESH
        )
    for rel in range(1, ny):
        pl.semaphore_signal(
            barrier, inc=1, device_id=(z, x, at_y(rel), c), device_id_type=pl.DeviceIdType.MESH
        )
    pl.semaphore_signal(barrier, inc=1, device_id=partner, device_id_type=pl.DeviceIdType.MESH)

    def lane_block(j):
        return pl.ds(pl.multiple_of(j * L, L), L)

    pltpu.make_async_copy(res_hbm.at[:, lane_block(me_j)], res, loc_sem.at[0]).start()
    for rel in range(ny):
        for side in range(2):
            j = 2 * at_y(rel) + (c if side == 0 else 1 - c)
            pltpu.make_async_copy(
                wo_hbm.at[:, lane_block(j)], wo.at[rel, :, pl.ds(side * L, L)], loc_sem.at[1]
            ).start()
    pltpu.make_async_copy(wg_hbm.at[0], wg, loc_sem.at[2]).start()
    pltpu.make_async_copy(wu_hbm.at[0], wu, loc_sem.at[3]).start()
    for rel in range(ny):
        for side in range(2):
            j = 2 * at_y(rel) + (c if side == 0 else 1 - c)
            pltpu.make_async_copy(
                wd_hbm.at[0, :, lane_block(j)], wd.at[rel, :, pl.ds(side * L, L)], loc_sem.at[4]
            ).start()

    lanes = lax.broadcasted_iota(jnp.int32, (T, L), 1)
    subs = lax.broadcasted_iota(jnp.int32, (T, L), 0)
    chosen = routes_ref[...]
    e0, e1 = chosen[:, 0:1], chosen[:, 1:2]
    m0, m1 = e0 == lanes, e1 == lanes
    member = jnp.where(m0 | m1, 1.0, 0.0).astype(BF)
    lower = jnp.where(lanes < subs, 1.0, 0.0).astype(BF)
    before = dot(lower, member)
    rank0 = jnp.sum(jnp.where(m0, before, 0.0), axis=1, keepdims=True)
    rank1 = jnp.sum(jnp.where(m1, before, 0.0), axis=1, keepdims=True)
    slot_ids = lax.broadcasted_iota(jnp.int32, (T, slots), 1).astype(F32)
    p0 = jnp.where(slot_ids == e0.astype(F32) * cap + rank0, 1.0, 0.0)
    p1 = jnp.where(slot_ids == e1.astype(F32) * cap + rank1, 1.0, 0.0)
    p0_ref[...] = p0.astype(BF)
    p1_ref[...] = p1.astype(BF)
    pick_ref[...] = jnp.transpose(p0 + p1).astype(BF)

    dist = (subs - lanes).astype(F32)
    q = q_ref[...]
    k = k_ref[...]
    head = 2 * me_j

    def masked(h, keys, gap, allowed):
        s = dot(q[:, h * HEAD_DIM : (h + 1) * HEAD_DIM], keys, ((1,), (1,)))
        idx = jnp.full((T, L), head + h + 1, jnp.int32).astype(F32)
        slope = jnp.exp2(-8.0 * idx / QH)
        return jnp.where(allowed, s * HEAD_DIM**-0.5 - slope * gap, -1e30)

    own_s = [masked(h, k, dist, lanes <= subs) for h in range(2)]

    pl.semaphore_wait(barrier, ns + ny - 1)

    nxt = lax.rem(me_s + 1, ns)
    after = (nxt // nx, lax.rem(nxt, nx), y, c)
    remote(k_ref, halo.at[0], send_sem.at[0], halo_sem.at[0], after)
    remote(v_ref, halo.at[1], send_sem.at[1], halo_sem.at[1], after)

    take(halo.at[0], halo_sem.at[0])
    take(halo.at[1], halo_sem.at[1])
    v_own = v_ref[...]
    v_old = halo[1]
    parts = []
    for h in range(2):
        old_s = masked(h, halo[0], dist + T, (lanes >= subs) & (me_s > 0))
        peak = jnp.maximum(
            jnp.max(own_s[h], axis=1, keepdims=True), jnp.max(old_s, axis=1, keepdims=True)
        )
        total = jnp.sum(jnp.exp(own_s[h] - peak), axis=1, keepdims=True) + jnp.sum(
            jnp.exp(old_s - peak), axis=1, keepdims=True
        )
        log_total = peak + jnp.log(total)
        mixed = dot(jnp.exp(own_s[h] - log_total).astype(BF), v_own) + dot(
            jnp.exp(old_s - log_total).astype(BF), v_old
        )
        keep = 1.0 / (1.0 + jnp.exp(sink_ref[h] - log_total))
        parts.append((mixed * keep).astype(BF))
    attended = jnp.concatenate(parts, axis=1)

    rels = [half]
    for d in range(half - 1, 0, -1):
        rels += [d, ny - d]
    rels += [0]
    take(wo, loc_sem.at[1])
    for rel in rels:
        o = dot(attended, wo[rel])
        own1[rel] = o[:, :L]
        ps1[rel] = o[:, L:].astype(BF)
        remote(ps1.at[rel], pr1.at[rel], send_sem.at[2], p1_sem.at[rel], partner)
    for rel in rels[:-1]:
        take(pr1.at[rel], p1_sem.at[rel])
        r1s[rel] = (own1[rel] + pr1[rel].astype(F32)).astype(BF)
        remote(r1s.at[rel], r1r.at[rel], send_sem.at[3], r1_sem.at[rel], (z, x, at_y(rel), c))
    take(pr1.at[0], p1_sem.at[0])
    take(res, loc_sem.at[0])
    total = res[...].astype(F32) + own1[0] + pr1[0].astype(F32)
    for rel in rels[-2::-1]:
        take(r1r.at[rel], r1_sem.at[rel])
        total = total + r1r[rel].astype(F32)
    state = total.astype(BF)
    state_ref[...] = state

    disp[...] = dot(pick_ref[...], state).astype(BF).reshape(ns, cap, L)
    for p in range(1, ns):
        tz, tx = sp_at(*pos[p])
        remote(
            disp.at[tz * nx + tx],
            ag.at[me_j, p],
            send_sem.at[4],
            disp_sem.at[p // per],
            (tz, tx, y, c),
        )
    ag[me_j, 0] = disp[me_s]

    def grp(g):
        return pl.ds(g * per, per)

    def hops(way, g):
        return half if (way == 0) == (g % 2 == 0) else half - 1

    def side_of(way):
        return (z, x, at_y(1 if way == 0 else -1), c)

    def pass_on(g, way, hop, j):
        if hop < hops(way, g):
            remote(
                ag.at[j, grp(g)],
                ag.at[j, grp(g)],
                send_sem.at[5],
                agr_sem.at[way, hop, g],
                side_of(way),
            )

    def across(g, j, rel):
        remote(ag.at[j, grp(g)], ag.at[j, grp(g)], send_sem.at[6], agd_sem.at[rel], partner)

    for g in range(G):
        if g == 0:
            take(ag.at[me_j, pl.ds(1, per - 1)], disp_sem.at[0])
        else:
            take(ag.at[me_j, grp(g)], disp_sem.at[g])
        for way in range(2):
            pass_on(g, way, 0, me_j)
        across(g, me_j, 0)

    take(wg, loc_sem.at[2])
    take(wu, loc_sem.at[3])

    def absorb(rel, first=False):
        yy = at_y(rel)
        take(ag.at[2 * yy + 1 - c], agd_sem.at[rel])
        cols = pl.ds(pl.multiple_of(yy * 2 * L, 2 * L), 2 * L)
        gain = gain_ref[:, cols]
        w_g, w_u = wg[cols, :], wu[cols, :]
        for g in range(G):
            at = pl.ds(g * rows, rows)
            lo = ag[2 * yy, grp(g)].reshape(rows, L).astype(F32)
            hi = ag[2 * yy + 1, grp(g)].reshape(rows, L).astype(F32)
            lhs = jnp.concatenate(
                [(lo * gain[:, :L]).astype(BF), (hi * gain[:, L:]).astype(BF)], axis=1
            )
            square = lo * lo + hi * hi
            if first:
                ssq[at, :] = square
                acc_g[at, :] = dot(lhs, w_g)
                acc_u[at, :] = dot(lhs, w_u)
            else:
                ssq[at, :] += square
                acc_g[at, :] += dot(lhs, w_g)
                acc_u[at, :] += dot(lhs, w_u)

    for hop in range(half):
        for g in range(G):
            for way in range(2):
                if hop < hops(way, g):
                    rel = ny - hop - 1 if way == 0 else hop + 1
                    j = 2 * at_y(rel) + c
                    take(ag.at[j, grp(g)], agr_sem.at[way, hop, g])
                    pass_on(g, way, hop + 1, j)
                    across(g, j, rel)
        if hop == 0:
            absorb(0, True)
        else:
            absorb(hop)
            absorb(ny - hop)
    absorb(half)

    for g in range(G):
        at = pl.ds(g * rows, rows)
        scale = lax.rsqrt(jnp.sum(ssq[at, :], axis=1, keepdims=True) / (2 * ny * L) + 1e-06)
        gate = acc_g[at, :] * scale
        act_ref[at, :] = (gate / (1.0 + jnp.exp(-gate)) * (acc_u[at, :] * scale)).astype(BF)

    take(wd, loc_sem.at[4])
    act = act_ref[...]
    for rel in rels:
        o = dot(act, wd[rel])
        own2[rel] = o[:, :L]
        ps2[rel] = o[:, L:].astype(BF)
        remote(ps2.at[rel], pr2.at[rel], send_sem.at[7], p2_sem.at[rel], partner)

    for stage in range(half):
        rel_of = (half - stage, (ny - half + stage) % ny)
        for rel in sorted(set(rel_of)):
            take(pr2.at[rel], p2_sem.at[rel])
        for g in reversed(range(G)):
            at = pl.ds(g * rows, rows)
            for way in range(2):
                begin = half - hops(way, g)
                if stage < begin:
                    continue
                rel = rel_of[way]
                s = own2[rel, at, :] + pr2[rel, at, :].astype(F32)
                if stage > begin:
                    take(r2r.at[way, stage - 1, g], r2_sem.at[way, stage - 1, g])
                    s = s + r2r[way, stage - 1, g].astype(F32)
                r2s[way, stage, g] = s.astype(BF)
                remote(
                    r2s.at[way, stage, g],
                    r2r.at[way, stage, g],
                    send_sem.at[8],
                    r2_sem.at[way, stage, g],
                    side_of(way),
                )
    take(pr2.at[0], p2_sem.at[0])
    for g in reversed(range(G)):
        at = pl.ds(g * rows, rows)
        s = own2[0, at, :] + pr2[0, at, :].astype(F32)
        for way in range(2):
            take(r2r.at[way, half - 1, g], r2_sem.at[way, half - 1, g])
            s = s + r2r[way, half - 1, g].astype(F32)
        out2[grp(g)] = s.astype(BF).reshape(per, cap, L)
        for p in reversed(range(g * per, (g + 1) * per)):
            if p == 0:
                ret[me_s] = out2[0]
                continue
            tz, tx = sp_at(-pos[p][0], -pos[p][1])
            remote(out2.at[p], ret.at[me_s], send_sem.at[9], ret_sem.at[0], (tz, tx, y, c))

    take(ret.at[pl.ds(0, ns - 1)], ret_sem.at[0])
    back = ret[...].reshape(slots, L)
    mix = rw_ref[:, 0:1] * dot(p0_ref[...], back) + rw_ref[:, 1:2] * dot(p1_ref[...], back)
    fin[me_j] = (state_ref[...].astype(F32) + mix).astype(BF)

    def write(j):
        pltpu.make_async_copy(fin.at[j], out_hbm.at[:, lane_block(j)], loc_sem.at[5]).start()

    for rel in rels[:-1]:
        remote(fin.at[me_j], fin.at[me_j], send_sem.at[10], fin_sem.at[rel], (z, x, at_y(rel), c))
    remote(fin.at[me_j], fin.at[me_j], send_sem.at[11], find_sem.at[0], partner)
    write(me_j)
    for rel in rels[-2::-1]:
        j = 2 * at_y(-rel) + c
        take(fin.at[j], fin_sem.at[rel])
        remote(fin.at[j], fin.at[j], send_sem.at[11], find_sem.at[rel], partner)
        write(j)
    for rel in rels[::-1]:
        j = 2 * at_y(-rel) + 1 - c
        take(fin.at[j], find_sem.at[rel])
        write(j)

    take(k_ref, send_sem.at[0])
    take(v_ref, send_sem.at[1])
    take(ps1, send_sem.at[2])
    take(r1s.at[pl.ds(0, ny - 1)], send_sem.at[3])
    take(disp.at[pl.ds(0, ns - 1)], send_sem.at[4])
    take(ag.at[pl.ds(0, ny - 1)], send_sem.at[5])
    take(ag.at[pl.ds(0, ny)], send_sem.at[6])
    take(ps2, send_sem.at[7])
    take(ps2.at[pl.ds(0, ny - 1)], send_sem.at[8])
    take(out2.at[pl.ds(0, ns - 1)], send_sem.at[9])
    take(fin.at[pl.ds(0, ny - 1)], send_sem.at[10])
    take(fin.at[pl.ds(0, ny)], send_sem.at[11])
    take(out_hbm, loc_sem.at[5])


def per_device(
    dims,
    queries,
    key_rows,
    value_rows,
    sink_logits,
    out_weight,
    residual,
    norm_gain,
    routes,
    route_weights,
    gate_weight,
    up_weight,
    down_weight,
):
    nz, nx, ny = dims
    ns = nz * nx
    width = residual.shape[1]
    hidden = gate_weight.shape[2]
    cap = 2 * T * TOP // ns
    slots = ns * cap
    rows = slots // G
    half = ny // 2
    vm = pl.BlockSpec(memory_space=pltpu.VMEM)
    hbm = pl.BlockSpec(memory_space=pl.ANY)
    sm = pl.BlockSpec(memory_space=pltpu.SMEM)
    scratch = [
        pltpu.VMEM((ny, T, 2 * L), BF),
        pltpu.VMEM((width, hidden), BF),
        pltpu.VMEM((width, hidden), BF),
        pltpu.VMEM((ny, hidden, 2 * L), BF),
        pltpu.VMEM((T, L), BF),
        pltpu.VMEM((2, T, HEAD_DIM), BF),
        pltpu.VMEM((T, slots), BF),
        pltpu.VMEM((T, slots), BF),
        pltpu.VMEM((slots, T), BF),
        pltpu.VMEM((ny, T, L), F32),
        pltpu.VMEM((ny, T, L), BF),
        pltpu.VMEM((ny, T, L), BF),
        pltpu.VMEM((ny, T, L), BF),
        pltpu.VMEM((ny, T, L), BF),
        pltpu.VMEM((T, L), BF),
        pltpu.VMEM((ns, cap, L), BF),
        pltpu.VMEM((2 * ny, ns, cap, L), BF),
        pltpu.VMEM((slots, hidden), F32),
        pltpu.VMEM((slots, hidden), F32),
        pltpu.VMEM((slots, L), F32),
        pltpu.VMEM((slots, hidden), BF),
        pltpu.VMEM((ny, slots, L), F32),
        pltpu.VMEM((ny, slots, L), BF),
        pltpu.VMEM((ny, slots, L), BF),
        pltpu.VMEM((2, half, G, rows, L), BF),
        pltpu.VMEM((2, half, G, rows, L), BF),
        pltpu.VMEM((ns, cap, L), BF),
        pltpu.VMEM((ns, cap, L), BF),
        pltpu.VMEM((2 * ny, T, L), BF),
        pltpu.SemaphoreType.DMA((6,)),
        pltpu.SemaphoreType.DMA((12,)),
        pltpu.SemaphoreType.DMA((2,)),
        pltpu.SemaphoreType.DMA((ny,)),
        pltpu.SemaphoreType.DMA((ny,)),
        pltpu.SemaphoreType.DMA((G,)),
        pltpu.SemaphoreType.DMA((2, half, G)),
        pltpu.SemaphoreType.DMA((ny,)),
        pltpu.SemaphoreType.DMA((ny,)),
        pltpu.SemaphoreType.DMA((2, half, G)),
        pltpu.SemaphoreType.DMA((1,)),
        pltpu.SemaphoreType.DMA((ny,)),
        pltpu.SemaphoreType.DMA((ny,)),
    ]
    return pl.pallas_call(
        functools.partial(layer, dims),
        out_shape=jax.ShapeDtypeStruct((T, width), BF),
        in_specs=[vm, vm, vm, sm, hbm, hbm, vm, vm, vm, hbm, hbm, hbm],
        out_specs=hbm,
        scratch_shapes=scratch,
        compiler_params=pltpu.CompilerParams(
            collective_id=0, has_side_effects=True, vmem_limit_bytes=48 * 1024 * 1024
        ),
        name="layer",
    )(
        queries,
        key_rows,
        value_rows,
        sink_logits,
        out_weight,
        residual,
        norm_gain.reshape(1, width),
        routes,
        route_weights,
        gate_weight,
        up_weight,
        down_weight,
    )


def build(devices, dims):
    torus = Mesh(devices.reshape(*dims, 2), ("z", "x", "y", "c"))
    sp, tp = ("z", "x"), ("y", "c")
    placed = (
        P(sp, tp),
        P(sp, tp),
        P(sp, tp),
        P(tp),
        P(tp, None),
        P(sp, None),
        P(),
        P(sp, None),
        P(sp, None),
        P(sp, None, tp),
        P(sp, None, tp),
        P(sp, tp, None),
    )
    return jax.shard_map(
        functools.partial(per_device, dims),
        mesh=torus,
        in_specs=placed,
        out_specs=P(sp, None),
        check_vma=False,
    )


def solution(mesh):
    sp, tp = mesh.shape["sp"], mesh.shape["tp"]
    return build(mesh.devices, (sp // NX, NX, tp // 2))
```

time: 253 us -> 94.7 us (0.37)
  blocking collectives: 150 us -> 0 us
  Pallas kernels: 0 us -> 84.7 us
  waiting for transfers between devices: 47.8 us -> 0 us
  starting transfers between devices: 14.5 us -> 0 us
  other arithmetic: 11.2 us -> 0 us
  matrix products: 10.5 us -> 0 us
  local copies, waits for them, and re-layouts: 18.1 us -> 9.5 us
    all_to_all x8 -> x0, blocking collectives: 150 us -> none  [the longest x2 62.3 us: summed_on_arrival(): lax.all_to_all(pieces, axis, split_axis=0, concat_axis=0, tiled=True)]
    pallas_call x0 -> x1, Pallas kernels: none -> 84.7 us  [per_device(): pl.pallas_call(functools.partial(layer, dims), out_shape=jax.ShapeDtypeSt...]
    all_to_all x3 -> x0, waiting for transfers between devices: 47.8 us -> none  [the longest x2 37.5 us: from_everyone(): return lax.all_to_all(copies, axis, split_axis=0, concat_axis=0, tiled=True)]
    all_to_all x3 -> x0, starting transfers between devices: 10.6 us -> none  [the longest x2 6.97 us: from_everyone(): return lax.all_to_all(copies, axis, split_axis=0, concat_axis=0, tiled=True)]
    dot_general x6 -> x0, matrix products: 10.5 us -> none  [the longest x1 5.02 us: per_device(): result = jnp.dot(activated, w_down, preferred_element_type=jnp.float32)]
    unnamed x25 -> x27, local copies, waits for them, and re-layouts: 2.49 us -> 9.5 us
    reduce_sum x9 -> x0, other arithmetic: 6.46 us -> none  [the longest x1 4.08 us: per_device(): jnp.sum(route_weights[..., None] * picked.astype(jnp.float32), axis=1)]
    gather x2 -> x0, local copies, waits for them, and re-layouts: 4.15 us -> none  [per_device(): jnp.take(slot_table, slot_index, axis=0).reshape(rows_here, TOP, width)]
  transfers between devices with their start and end apart: 4 -> 0, of which waited for: 3 -> 0; matrix products, arithmetic and copies ran while one was open for 1% -> 0% of each run, Pallas kernels for 0% -> 0%
where the time goes in v1:
time: 94.7 us; the launch traced here: 94.3 us
  Pallas kernels  84.7 us (89%)
  local copies, waits for them, and re-layouts  9.5 us (10%)
    pallas_call x1, Pallas kernels, per_device(): pl.pallas_call(functools.partial(layer, dims), out_shape=jax.ShapeDtypeSt...  84.7 us
    unnamed x27, local copies, waits for them, and re-layouts  9.5 us

profile of v1, /device:TPU:1, one launch (start us, length us, event | category | flops | bytes accessed | tf_op | source)
XLA Modules:
  0.0 94.3 jit_solution(16744789043465099009)
XLA Ops:
  0.0 0.0 copy-start.8
  0.0 0.8 copy.13.k_ref
  0.8 0.0 copy-done.8
  0.9 0.0 copy-start.9
  0.9 0.1 copy.14.v_ref
  1.0 0.6 copy-done.9
  1.5 0.0 copy-start.10
  1.5 0.1 copy.15.routes_ref
  1.6 0.6 copy-done.10
  2.2 0.0 copy-start.5
  2.2 0.0 copy-start.6
  2.2 0.0 copy-start.7
  2.2 0.1 copy.16.rw_ref
  2.3 0.6 copy-done.5
  3.0 0.0 copy-done.6
  3.0 0.0 copy-done.7
  3.0 0.0 copy-start
  3.0 1.2 %copy-done = bf16[1,2048,256]{2,1,0:T(8,128)(2,1)S(1)} copy-done((bf16[1,2048,256]{2,1,0:T(8,128)(2,1)S(1)}, bf16[1,2048,256]{2,1,0:T(8,128)(2,1)}, u32[]{:S(2)}) %copy-start) | copy-done | bytes 1048600
  4.2 0.0 copy-start.1
  4.2 1.2 %copy-done.1 = bf16[1,2048,256]{2,1,0:T(8,128)(2,1)S(1)} copy-done((bf16[1,2048,256]{2,1,0:T(8,128)(2,1)S(1)}, bf16[1,2048,256]{2,1,0:T(8,128)(2,1)}, u32[]{:S(2)}) %copy-start.1) | copy-done | bytes 1048600
  5.4 0.0 copy-start.2
  5.4 1.2 %copy-done.2 = bf16[1,256,2048]{2,1,0:T(8,128)(2,1)S(1)} copy-done((bf16[1,256,2048]{2,1,0:T(8,128)(2,1)S(1)}, bf16[1,256,2048]{2,1,0:T(8,128)(2,1)}, u32[]{:S(2)}) %copy-start.2) | copy-done | bytes 1048600
  6.7 0.0 copy-start.3
  6.7 1.0 %copy-done.3 = bf16[128,2048]{1,0:T(8,128)(2,1)S(1)} copy-done((bf16[128,2048]{1,0:T(8,128)(2,1)S(1)}, bf16[128,2048]{1,0:T(8,128)(2,1)}, u32[]{:S(2)}) %copy-start.3) | copy-done | bytes 524312
  7.7 0.0 copy-start.4
  7.7 1.0 %copy-done.4 = bf16[128,2048]{1,0:T(8,128)(2,1)S(1)} copy-done((bf16[128,2048]{1,0:T(8,128)(2,1)S(1)}, bf16[128,2048]{1,0:T(8,128)(2,1)}, u32[]{:S(2)}) %copy-start.4) | copy-done | bytes 524312
  8.7 84.7 %layer.1 = bf16[128,2048]{1,0:T(8,128)(2,1)S(1)} custom-call(bf16[128,128]{1,0:T(8,128)(2,1)S(1)} %copy-done.5, bf16[128,64]{1,0:T(8,128)(2,1)S(1)} %copy.13.k_ref, bf16[128,64]{1,0:T(8,128)(2,1)S(1)} %copy.14.v_ref, f32[2]{0:T(128)S(1)} %copy-done.7, bf16[128,2048]{1,0:T(8,128)(2,1)S(1)} %copy-done.3, bf16[128,2048]{1,0:T(8,128)(2,1)S(1)} %copy-done.4, ...), custom_call_target="tpu_custom_call" | custom-call | tf_op jit(solution)/shard_map/layer/pallas_call | solution.py:482
  93.5 0.8 copy.18
Async XLA Ops:
  0.0 0.8 copy-start.8
  0.9 0.7 copy-start.9
  1.5 0.7 copy-start.10
  2.2 0.8 copy-start.5
  2.2 0.8 copy-start.6
  2.2 0.8 copy-start.7
  3.0 1.2 %copy-start = (bf16[1,2048,256]{2,1,0:T(8,128)(2,1)S(1)}, bf16[1,2048,256]{2,1,0:T(8,128)(2,1)}, u32[]{:S(2)}) copy-start(bf16[1,2048,256]{2,1,0:T(8,128)(2,1)} %wg_hbm.1) | copy-start | bytes 3145732
  4.2 1.2 %copy-start.1 = (bf16[1,2048,256]{2,1,0:T(8,128)(2,1)S(1)}, bf16[1,2048,256]{2,1,0:T(8,128)(2,1)}, u32[]{:S(2)}) copy-start(bf16[1,2048,256]{2,1,0:T(8,128)(2,1)} %wu_hbm.1) | copy-start | bytes 3145732
  5.4 1.2 %copy-start.2 = (bf16[1,256,2048]{2,1,0:T(8,128)(2,1)S(1)}, bf16[1,256,2048]{2,1,0:T(8,128)(2,1)}, u32[]{:S(2)}) copy-start(bf16[1,256,2048]{2,1,0:T(8,128)(2,1)} %wd_hbm.1) | copy-start | bytes 3145732
  6.7 1.0 %copy-start.3 = (bf16[128,2048]{1,0:T(8,128)(2,1)S(1)}, bf16[128,2048]{1,0:T(8,128)(2,1)}, u32[]{:S(2)}) copy-start(bf16[128,2048]{1,0:T(8,128)(2,1)} %wo_hbm.1) | copy-start | bytes 1572868
  7.7 1.0 %copy-start.4 = (bf16[128,2048]{1,0:T(8,128)(2,1)S(1)}, bf16[128,2048]{1,0:T(8,128)(2,1)}, u32[]{:S(2)}) copy-start(bf16[128,2048]{1,0:T(8,128)(2,1)} %res_hbm.1) | copy-start | bytes 1572868

commit v2 on v1

--- a/solution.py
+++ b/solution.py
@@ -33,19 +33,25 @@
 
 def layer(
     dims,
-    q_ref,
-    k_ref,
-    v_ref,
+    q_hbm,
+    k_hbm,
+    v_hbm,
     sink_ref,
     wo_hbm,
     res_hbm,
-    gain_ref,
-    routes_ref,
-    rw_ref,
+    gain_hbm,
+    routes_hbm,
+    rw_hbm,
     wg_hbm,
     wu_hbm,
     wd_hbm,
     out_hbm,
+    q_ref,
+    kv_ref,
+    gain_ref,
+    routes_ref,
+    rw_ref,
+    rate_ref,
     wo,
     wg,
     wu,
@@ -138,62 +144,84 @@
     def lane_block(j):
         return pl.ds(pl.multiple_of(j * L, L), L)
 
-    pltpu.make_async_copy(res_hbm.at[:, lane_block(me_j)], res, loc_sem.at[0]).start()
+    loads = {}
+
+    def load(name, src, dst, sem):
+        pltpu.make_async_copy(src, dst, loc_sem.at[sem]).start()
+        loads[name] = (dst, loc_sem.at[sem])
+
+    def ready(name):
+        take(*loads.pop(name))
+
+    pending = []
+
+    load("k", k_hbm, kv_ref.at[0], 6)
+    load("v", v_hbm, kv_ref.at[1], 7)
+    load("q", q_hbm, q_ref, 8)
+    load("routes", routes_hbm, routes_ref, 9)
+    load("rw", rw_hbm, rw_ref, 10)
+    load("gain", gain_hbm, gain_ref, 11)
+    load("res", res_hbm.at[:, lane_block(me_j)], res, 0)
     for rel in range(ny):
         for side in range(2):
             j = 2 * at_y(rel) + (c if side == 0 else 1 - c)
             pltpu.make_async_copy(
                 wo_hbm.at[:, lane_block(j)], wo.at[rel, :, pl.ds(side * L, L)], loc_sem.at[1]
             ).start()
-    pltpu.make_async_copy(wg_hbm.at[0], wg, loc_sem.at[2]).start()
-    pltpu.make_async_copy(wu_hbm.at[0], wu, loc_sem.at[3]).start()
+    loads["wo"] = (wo, loc_sem.at[1])
+    load("wg", wg_hbm.at[0], wg, 2)
+    load("wu", wu_hbm.at[0], wu, 3)
     for rel in range(ny):
         for side in range(2):
             j = 2 * at_y(rel) + (c if side == 0 else 1 - c)
             pltpu.make_async_copy(
                 wd_hbm.at[0, :, lane_block(j)], wd.at[rel, :, pl.ds(side * L, L)], loc_sem.at[4]
             ).start()
-
+    loads["wd"] = (wd, loc_sem.at[4])
+
+    ready("routes")
+    ready("rw")
     lanes = lax.broadcasted_iota(jnp.int32, (T, L), 1)
     subs = lax.broadcasted_iota(jnp.int32, (T, L), 0)
-    chosen = routes_ref[...]
-    e0, e1 = chosen[:, 0:1], chosen[:, 1:2]
-    m0, m1 = e0 == lanes, e1 == lanes
-    member = jnp.where(m0 | m1, 1.0, 0.0).astype(BF)
-    lower = jnp.where(lanes < subs, 1.0, 0.0).astype(BF)
-    before = dot(lower, member)
-    rank0 = jnp.sum(jnp.where(m0, before, 0.0), axis=1, keepdims=True)
-    rank1 = jnp.sum(jnp.where(m1, before, 0.0), axis=1, keepdims=True)
-    slot_ids = lax.broadcasted_iota(jnp.int32, (T, slots), 1).astype(F32)
-    p0 = jnp.where(slot_ids == e0.astype(F32) * cap + rank0, 1.0, 0.0)
-    p1 = jnp.where(slot_ids == e1.astype(F32) * cap + rank1, 1.0, 0.0)
-    p0_ref[...] = p0.astype(BF)
-    p1_ref[...] = p1.astype(BF)
-    pick_ref[...] = jnp.transpose(p0 + p1).astype(BF)
+    experts = lax.broadcasted_iota(jnp.int32, (ns, T), 0)
+    slot_ids = lax.broadcasted_iota(jnp.int32, (slots, T), 0).astype(F32)
+    earlier = jnp.where(subs < lanes, 1.0, 0.0).astype(BF)
+    chosen = [routes_ref[t : t + 1, :] for t in range(TOP)]
+    named = [e == experts for e in chosen]
+    member = jnp.where(named[0] | named[1], 1.0, 0.0).astype(BF)
+    before = dot(member, earlier)
+    picks = []
+    for t in range(TOP):
+        rank = jnp.sum(jnp.where(named[t], before, 0.0), axis=0, keepdims=True)
+        picks.append(jnp.where(slot_ids == chosen[t].astype(F32) * cap + rank, 1.0, 0.0))
+        rate_ref[t] = jnp.transpose(jnp.broadcast_to(rw_ref[t : t + 1, :], (L, T)))
+    p0_ref[...] = jnp.transpose(picks[0]).astype(BF)
+    p1_ref[...] = jnp.transpose(picks[1]).astype(BF)
+    pick_ref[...] = (picks[0] + picks[1]).astype(BF)
 
     dist = (subs - lanes).astype(F32)
+    ready("q")
+    ready("k")
+    ready("v")
     q = q_ref[...]
-    k = k_ref[...]
     head = 2 * me_j
 
     def masked(h, keys, gap, allowed):
-        s = dot(q[:, h * HEAD_DIM : (h + 1) * HEAD_DIM], keys, ((1,), (1,)))
+        s = dot(q[:, h * HEAD_DIM : (h + 1) * HEAD_DIM], keys)
         idx = jnp.full((T, L), head + h + 1, jnp.int32).astype(F32)
         slope = jnp.exp2(-8.0 * idx / QH)
         return jnp.where(allowed, s * HEAD_DIM**-0.5 - slope * gap, -1e30)
 
-    own_s = [masked(h, k, dist, lanes <= subs) for h in range(2)]
+    own_s = [masked(h, kv_ref[0], dist, lanes <= subs) for h in range(2)]
 
     pl.semaphore_wait(barrier, ns + ny - 1)
 
     nxt = lax.rem(me_s + 1, ns)
     after = (nxt // nx, lax.rem(nxt, nx), y, c)
-    remote(k_ref, halo.at[0], send_sem.at[0], halo_sem.at[0], after)
-    remote(v_ref, halo.at[1], send_sem.at[1], halo_sem.at[1], after)
-
-    take(halo.at[0], halo_sem.at[0])
-    take(halo.at[1], halo_sem.at[1])
-    v_own = v_ref[...]
+    remote(kv_ref, halo, send_sem.at[0], halo_sem.at[0], after)
+    pending.append((kv_ref, send_sem.at[0]))
+    take(halo, halo_sem.at[0])
+    v_own = kv_ref[1]
     v_old = halo[1]
     parts = []
     for h in range(2):
@@ -205,8 +233,8 @@
             jnp.exp(old_s - peak), axis=1, keepdims=True
         )
         log_total = peak + jnp.log(total)
-        mixed = dot(jnp.exp(own_s[h] - log_total).astype(BF), v_own) + dot(
-            jnp.exp(old_s - log_total).astype(BF), v_old
+        mixed = dot(jnp.exp(own_s[h] - log_total).astype(BF), v_own, ((1,), (1,))) + dot(
+            jnp.exp(old_s - log_total).astype(BF), v_old, ((1,), (1,))
         )
         keep = 1.0 / (1.0 + jnp.exp(sink_ref[h] - log_total))
         parts.append((mixed * keep).astype(BF))
@@ -216,18 +244,20 @@
     for d in range(half - 1, 0, -1):
         rels += [d, ny - d]
     rels += [0]
-    take(wo, loc_sem.at[1])
+    ready("wo")
     for rel in rels:
         o = dot(attended, wo[rel])
         own1[rel] = o[:, :L]
         ps1[rel] = o[:, L:].astype(BF)
         remote(ps1.at[rel], pr1.at[rel], send_sem.at[2], p1_sem.at[rel], partner)
+    pending.append((ps1, send_sem.at[2]))
     for rel in rels[:-1]:
         take(pr1.at[rel], p1_sem.at[rel])
         r1s[rel] = (own1[rel] + pr1[rel].astype(F32)).astype(BF)
         remote(r1s.at[rel], r1r.at[rel], send_sem.at[3], r1_sem.at[rel], (z, x, at_y(rel), c))
+    pending.append((r1s.at[pl.ds(0, ny - 1)], send_sem.at[3]))
     take(pr1.at[0], p1_sem.at[0])
-    take(res, loc_sem.at[0])
+    ready("res")
     total = res[...].astype(F32) + own1[0] + pr1[0].astype(F32)
     for rel in rels[-2::-1]:
         take(r1r.at[rel], r1_sem.at[rel])
@@ -246,6 +276,7 @@
             (tz, tx, y, c),
         )
     ag[me_j, 0] = disp[me_s]
+    pending.append((disp.at[pl.ds(0, ns - 1)], send_sem.at[4]))
 
     def grp(g):
         return pl.ds(g * per, per)
@@ -278,8 +309,9 @@
             pass_on(g, way, 0, me_j)
         across(g, me_j, 0)
 
-    take(wg, loc_sem.at[2])
-    take(wu, loc_sem.at[3])
+    ready("wg")
+    ready("wu")
+    ready("gain")
 
     def absorb(rel, first=False):
         yy = at_y(rel)
@@ -319,6 +351,8 @@
             absorb(hop)
             absorb(ny - hop)
     absorb(half)
+    pending.append((ag.at[pl.ds(0, ny - 1)], send_sem.at[5]))
+    pending.append((ag.at[pl.ds(0, ny)], send_sem.at[6]))
 
     for g in range(G):
         at = pl.ds(g * rows, rows)
@@ -326,7 +360,7 @@
         gate = acc_g[at, :] * scale
         act_ref[at, :] = (gate / (1.0 + jnp.exp(-gate)) * (acc_u[at, :] * scale)).astype(BF)
 
-    take(wd, loc_sem.at[4])
+    ready("wd")
     act = act_ref[...]
     for rel in rels:
         o = dot(act, wd[rel])
@@ -334,6 +368,7 @@
         ps2[rel] = o[:, L:].astype(BF)
         remote(ps2.at[rel], pr2.at[rel], send_sem.at[7], p2_sem.at[rel], partner)
 
+    pending.append((ps2, send_sem.at[7]))
     for stage in range(half):
         rel_of = (half - stage, (ny - half + stage) % ny)
         for rel in sorted(set(rel_of)):
@@ -372,9 +407,11 @@
             tz, tx = sp_at(-pos[p][0], -pos[p][1])
             remote(out2.at[p], ret.at[me_s], send_sem.at[9], ret_sem.at[0], (tz, tx, y, c))
 
+    pending.append((ps2.at[pl.ds(0, ny - 1)], send_sem.at[8]))
+    pending.append((out2.at[pl.ds(0, ns - 1)], send_sem.at[9]))
     take(ret.at[pl.ds(0, ns - 1)], ret_sem.at[0])
     back = ret[...].reshape(slots, L)
-    mix = rw_ref[:, 0:1] * dot(p0_ref[...], back) + rw_ref[:, 1:2] * dot(p1_ref[...], back)
+    mix = rate_ref[0] * dot(p0_ref[...], back) + rate_ref[1] * dot(p1_ref[...], back)
     fin[me_j] = (state_ref[...].astype(F32) + mix).astype(BF)
 
     def write(j):
@@ -394,19 +431,11 @@
         take(fin.at[j], find_sem.at[rel])
         write(j)
 
-    take(k_ref, send_sem.at[0])
-    take(v_ref, send_sem.at[1])
-    take(ps1, send_sem.at[2])
-    take(r1s.at[pl.ds(0, ny - 1)], send_sem.at[3])
-    take(disp.at[pl.ds(0, ns - 1)], send_sem.at[4])
-    take(ag.at[pl.ds(0, ny - 1)], send_sem.at[5])
-    take(ag.at[pl.ds(0, ny)], send_sem.at[6])
-    take(ps2, send_sem.at[7])
-    take(ps2.at[pl.ds(0, ny - 1)], send_sem.at[8])
-    take(out2.at[pl.ds(0, ns - 1)], send_sem.at[9])
-    take(fin.at[pl.ds(0, ny - 1)], send_sem.at[10])
-    take(fin.at[pl.ds(0, ny)], send_sem.at[11])
-    take(out_hbm, loc_sem.at[5])
+    pending.append((fin.at[pl.ds(0, ny - 1)], send_sem.at[10]))
+    pending.append((fin.at[pl.ds(0, ny)], send_sem.at[11]))
+    pending.append((out_hbm, loc_sem.at[5]))
+    for ref, sem in pending:
+        take(ref, sem)
 
 
 def per_device(
@@ -432,16 +461,21 @@
     slots = ns * cap
     rows = slots // G
     half = ny // 2
-    vm = pl.BlockSpec(memory_space=pltpu.VMEM)
     hbm = pl.BlockSpec(memory_space=pl.ANY)
     sm = pl.BlockSpec(memory_space=pltpu.SMEM)
     scratch = [
+        pltpu.VMEM((T, L), BF),
+        pltpu.VMEM((2, HEAD_DIM, T), BF),
+        pltpu.VMEM((1, width), F32),
+        pltpu.VMEM((TOP, T), jnp.int32),
+        pltpu.VMEM((TOP, T), F32),
+        pltpu.VMEM((TOP, T, L), F32),
         pltpu.VMEM((ny, T, 2 * L), BF),
         pltpu.VMEM((width, hidden), BF),
         pltpu.VMEM((width, hidden), BF),
         pltpu.VMEM((ny, hidden, 2 * L), BF),
         pltpu.VMEM((T, L), BF),
-        pltpu.VMEM((2, T, HEAD_DIM), BF),
+        pltpu.VMEM((2, HEAD_DIM, T), BF),
         pltpu.VMEM((T, slots), BF),
         pltpu.VMEM((T, slots), BF),
         pltpu.VMEM((slots, T), BF),
@@ -465,9 +499,9 @@
         pltpu.VMEM((ns, cap, L), BF),
         pltpu.VMEM((ns, cap, L), BF),
         pltpu.VMEM((2 * ny, T, L), BF),
-        pltpu.SemaphoreType.DMA((6,)),
         pltpu.SemaphoreType.DMA((12,)),
-        pltpu.SemaphoreType.DMA((2,)),
+        pltpu.SemaphoreType.DMA((12,)),
+        pltpu.SemaphoreType.DMA((1,)),
         pltpu.SemaphoreType.DMA((ny,)),
         pltpu.SemaphoreType.DMA((ny,)),
         pltpu.SemaphoreType.DMA((G,)),
@@ -482,23 +516,23 @@
     return pl.pallas_call(
         functools.partial(layer, dims),
         out_shape=jax.ShapeDtypeStruct((T, width), BF),
-        in_specs=[vm, vm, vm, sm, hbm, hbm, vm, vm, vm, hbm, hbm, hbm],
+        in_specs=[hbm, hbm, hbm, sm] + [hbm] * 8,
         out_specs=hbm,
         scratch_shapes=scratch,
         compiler_params=pltpu.CompilerParams(
-            collective_id=0, has_side_effects=True, vmem_limit_bytes=48 * 1024 * 1024
+            collective_id=0, has_side_effects=True, vmem_limit_bytes=67043328
         ),
         name="layer",
     )(
         queries,
-        key_rows,
-        value_rows,
+        key_rows.T,
+        value_rows.T,
         sink_logits,
         out_weight,
         residual,
         norm_gain.reshape(1, width),
-        routes,
-        route_weights,
+        routes.T,
+        route_weights.T,
         gate_weight,
         up_weight,
         down_weight,

time: 94.7 us -> 87.2 us (0.921)
  local copies, waits for them, and re-layouts: 9.5 us -> 1.88 us
    unnamed x27 -> x1, local copies, waits for them, and re-layouts: 9.5 us -> 1.88 us
where the time goes in v2:
time: 87.2 us; the launch traced here: 87 us
  Pallas kernels  85.1 us (98%)
  local copies, waits for them, and re-layouts  1.88 us (2%)
    pallas_call x1, Pallas kernels, per_device(): pl.pallas_call(functools.partial(layer, dims), out_shape=jax.ShapeDtypeSt...  85.1 us
    unnamed x1, local copies, waits for them, and re-layouts  1.88 us

profile of v2, /device:TPU:1, one launch (start us, length us, event | category | flops | bytes accessed | tf_op | source)
XLA Modules:
  0.0 87.0 jit_solution(10190251672728462399)
XLA Ops:
  0.0 85.1 %layer.1 = bf16[128,2048]{1,0:T(8,128)(2,1)} custom-call(bf16[128,128]{1,0:T(8,128)(2,1)} %q_hbm.1, bf16[64,128]{1,0:T(8,128)(2,1)} %bitcast.5, bf16[64,128]{1,0:T(8,128)(2,1)} %bitcast.6, f32[2]{0:T(128)} %sink_ref.1, bf16[128,2048]{1,0:T(8,128)(2,1)} %wo_hbm.1, bf16[128,2048]{1,0:T(8,128)(2,1)} %res_hbm.1, f32[1,2048]{1,0:T(1,128)} %bitcast.7, ...), custom_call_target="tpu_custom_call" | custom-call | tf_op jit(solution)/shard_map/layer/pallas_call | solution.py:516
  85.2 1.9 %copy.14 = bf16[128,2048]{1,0:T(8,128)(2,1)} copy(bf16[128,2048]{1,0:T(8,128)(2,1)} %layer.1) | data formatting | bytes 1048576

commit v3 on v2

--- a/solution.py
+++ b/solution.py
@@ -13,7 +13,8 @@
 TOP = 2
 T = 128
 L = 128
-G = 4
+G = 8
+HS = 2
 BF = jnp.bfloat16
 F32 = jnp.float32
 NX = 4
@@ -58,6 +59,7 @@
     wd,
     res,
     halo,
+    old_ref,
     p0_ref,
     p1_ref,
     pick_ref,
@@ -94,6 +96,7 @@
     ret_sem,
     fin_sem,
     find_sem,
+    know_sem,
 ):
     nz, nx, ny = dims
     ns = nz * nx
@@ -130,16 +133,36 @@
         pltpu.make_async_copy(ref, ref, sem).wait()
 
     barrier = pltpu.get_barrier_semaphore()
-    for dz, dx in pos[1:]:
-        tz, tx = sp_at(dz, dx)
-        pl.semaphore_signal(
-            barrier, inc=1, device_id=(tz, tx, y, c), device_id_type=pl.DeviceIdType.MESH
-        )
+
+    def along(d):
+        at = lax.rem(me_s + d + ns, ns)
+        return at // nx, lax.rem(at, nx), y, c
+
+    def signal(sem, dev):
+        pl.semaphore_signal(sem, inc=1, device_id=dev, device_id_type=pl.DeviceIdType.MESH)
+
+    signal(barrier, along(1))
+    signal(barrier, along(-1))
+    signal(barrier, partner)
     for rel in range(1, ny):
-        pl.semaphore_signal(
-            barrier, inc=1, device_id=(z, x, at_y(rel), c), device_id_type=pl.DeviceIdType.MESH
-        )
-    pl.semaphore_signal(barrier, inc=1, device_id=partner, device_id_type=pl.DeviceIdType.MESH)
+        signal(barrier, (z, x, at_y(rel), c))
+    shifts = [1 << i for i in range(know_sem.shape[0])]
+
+    def tell(i):
+        signal(know_sem.at[i], along(shifts[i]))
+        signal(know_sem.at[i], along(-shifts[i]))
+
+    def hear(i):
+        pl.semaphore_wait(know_sem.at[i], 2)
+        if i + 1 < len(shifts):
+            tell(i + 1)
+
+    heard = iter(range(len(shifts)))
+
+    def hear_next():
+        for i in heard:
+            hear(i)
+            return
 
     def lane_block(j):
         return pl.ds(pl.multiple_of(j * L, L), L)
@@ -214,18 +237,28 @@
 
     own_s = [masked(h, kv_ref[0], dist, lanes <= subs) for h in range(2)]
 
-    pl.semaphore_wait(barrier, ns + ny - 1)
-
-    nxt = lax.rem(me_s + 1, ns)
-    after = (nxt // nx, lax.rem(nxt, nx), y, c)
-    remote(kv_ref, halo, send_sem.at[0], halo_sem.at[0], after)
-    pending.append((kv_ref, send_sem.at[0]))
-    take(halo, halo_sem.at[0])
+    pl.semaphore_wait(barrier, ny + 2)
+    tell(0)
+
+    @pl.when(me_s < ns - 1)
+    def _():
+        remote(kv_ref, halo, send_sem.at[0], halo_sem.at[0], along(1))
+
+    @pl.when(me_s > 0)
+    def _():
+        take(halo, halo_sem.at[0])
+        old_ref[...] = halo[...]
+
+    @pl.when(me_s == 0)
+    def _():
+        old_ref[...] = kv_ref[...]
+
     v_own = kv_ref[1]
-    v_old = halo[1]
+    k_old = old_ref[0]
+    v_old = old_ref[1]
     parts = []
     for h in range(2):
-        old_s = masked(h, halo[0], dist + T, (lanes >= subs) & (me_s > 0))
+        old_s = masked(h, k_old, dist + T, (lanes >= subs) & (me_s > 0))
         peak = jnp.maximum(
             jnp.max(own_s[h], axis=1, keepdims=True), jnp.max(old_s, axis=1, keepdims=True)
         )
@@ -251,20 +284,26 @@
         ps1[rel] = o[:, L:].astype(BF)
         remote(ps1.at[rel], pr1.at[rel], send_sem.at[2], p1_sem.at[rel], partner)
     pending.append((ps1, send_sem.at[2]))
+    hear_next()
     for rel in rels[:-1]:
         take(pr1.at[rel], p1_sem.at[rel])
         r1s[rel] = (own1[rel] + pr1[rel].astype(F32)).astype(BF)
         remote(r1s.at[rel], r1r.at[rel], send_sem.at[3], r1_sem.at[rel], (z, x, at_y(rel), c))
     pending.append((r1s.at[pl.ds(0, ny - 1)], send_sem.at[3]))
+    hear_next()
     take(pr1.at[0], p1_sem.at[0])
     ready("res")
     total = res[...].astype(F32) + own1[0] + pr1[0].astype(F32)
-    for rel in rels[-2::-1]:
+    for i, rel in enumerate(rels[-2::-1]):
         take(r1r.at[rel], r1_sem.at[rel])
         total = total + r1r[rel].astype(F32)
+        if i == half:
+            hear_next()
     state = total.astype(BF)
     state_ref[...] = state
 
+    for i in heard:
+        hear(i)
     disp[...] = dot(pick_ref[...], state).astype(BF).reshape(ns, cap, L)
     for p in range(1, ns):
         tz, tx = sp_at(*pos[p])
@@ -298,7 +337,8 @@
             )
 
     def across(g, j, rel):
-        remote(ag.at[j, grp(g)], ag.at[j, grp(g)], send_sem.at[6], agd_sem.at[rel], partner)
+        at = ny if rel == half and g >= G // HS else rel
+        remote(ag.at[j, grp(g)], ag.at[j, grp(g)], send_sem.at[6], agd_sem.at[at], partner)
 
     for g in range(G):
         if g == 0:
@@ -313,73 +353,83 @@
     ready("wu")
     ready("gain")
 
-    def absorb(rel, first=False):
+    tall = slots // HS
+
+    def absorb(rel, hs):
         yy = at_y(rel)
-        take(ag.at[2 * yy + 1 - c], agd_sem.at[rel])
+        other = 2 * yy + 1 - c
+        part = pl.ds(hs * (ns // HS), ns // HS)
+        if rel == half:
+            take(ag.at[other, part], agd_sem.at[rel if hs == 0 else ny])
+        elif hs == 0:
+            take(ag.at[other], agd_sem.at[rel])
         cols = pl.ds(pl.multiple_of(yy * 2 * L, 2 * L), 2 * L)
         gain = gain_ref[:, cols]
-        w_g, w_u = wg[cols, :], wu[cols, :]
+        at = pl.ds(hs * tall, tall)
+        lo = ag[2 * yy, part].reshape(tall, L).astype(F32)
+        hi = ag[2 * yy + 1, part].reshape(tall, L).astype(F32)
+        lhs = jnp.concatenate(
+            [(lo * gain[:, :L]).astype(BF), (hi * gain[:, L:]).astype(BF)], axis=1
+        )
+        square = lo * lo + hi * hi
+        if rel == 0:
+            ssq[at, :] = square
+            acc_g[at, :] = dot(lhs, wg[cols, :])
+            acc_u[at, :] = dot(lhs, wu[cols, :])
+        else:
+            ssq[at, :] += square
+            acc_g[at, :] += dot(lhs, wg[cols, :])
+            acc_u[at, :] += dot(lhs, wu[cols, :])
+
+    def catch(g, way, hop):
+        rel = ny - hop - 1 if way == 0 else hop + 1
+        j = 2 * at_y(rel) + c
+        take(ag.at[j, grp(g)], agr_sem.at[way, hop, g])
+        pass_on(g, way, hop + 1, j)
+        across(g, j, rel)
+
+    todo = [(0, hs) for hs in range(HS)]
+    for hop in range(half - 1):
         for g in range(G):
-            at = pl.ds(g * rows, rows)
-            lo = ag[2 * yy, grp(g)].reshape(rows, L).astype(F32)
-            hi = ag[2 * yy + 1, grp(g)].reshape(rows, L).astype(F32)
-            lhs = jnp.concatenate(
-                [(lo * gain[:, :L]).astype(BF), (hi * gain[:, L:]).astype(BF)], axis=1
-            )
-            square = lo * lo + hi * hi
-            if first:
-                ssq[at, :] = square
-                acc_g[at, :] = dot(lhs, w_g)
-                acc_u[at, :] = dot(lhs, w_u)
-            else:
-                ssq[at, :] += square
-                acc_g[at, :] += dot(lhs, w_g)
-                acc_u[at, :] += dot(lhs, w_u)
-
-    for hop in range(half):
-        for g in range(G):
-            for way in range(2):
-                if hop < hops(way, g):
-                    rel = ny - hop - 1 if way == 0 else hop + 1
-                    j = 2 * at_y(rel) + c
-                    take(ag.at[j, grp(g)], agr_sem.at[way, hop, g])
-                    pass_on(g, way, hop + 1, j)
-                    across(g, j, rel)
-        if hop == 0:
-            absorb(0, True)
-        else:
-            absorb(hop)
-            absorb(ny - hop)
-    absorb(half)
-    pending.append((ag.at[pl.ds(0, ny - 1)], send_sem.at[5]))
-    pending.append((ag.at[pl.ds(0, ny)], send_sem.at[6]))
-
-    for g in range(G):
-        at = pl.ds(g * rows, rows)
+            catch(g, 0, hop)
+            catch(g, 1, hop)
+            if g % 2 == 1 and todo:
+                absorb(*todo.pop(0))
+        while todo:
+            absorb(*todo.pop(0))
+        todo = [(rel, hs) for rel in (ny - hop - 1, hop + 1) for hs in range(HS)]
+
+    def activate(hs):
+        at = pl.ds(hs * tall, tall)
         scale = lax.rsqrt(jnp.sum(ssq[at, :], axis=1, keepdims=True) / (2 * ny * L) + 1e-06)
         gate = acc_g[at, :] * scale
         act_ref[at, :] = (gate / (1.0 + jnp.exp(-gate)) * (acc_u[at, :] * scale)).astype(BF)
 
-    ready("wd")
-    act = act_ref[...]
-    for rel in rels:
-        o = dot(act, wd[rel])
-        own2[rel] = o[:, :L]
-        ps2[rel] = o[:, L:].astype(BF)
-        remote(ps2.at[rel], pr2.at[rel], send_sem.at[7], p2_sem.at[rel], partner)
-
-    pending.append((ps2, send_sem.at[7]))
-    for stage in range(half):
-        rel_of = (half - stage, (ny - half + stage) % ny)
-        for rel in sorted(set(rel_of)):
-            take(pr2.at[rel], p2_sem.at[rel])
-        for g in reversed(range(G)):
+    def project(hs):
+        at = pl.ds(hs * tall, tall)
+        act = act_ref[at, :]
+        for rel in rels:
+            o = dot(act, wd[rel])
+            own2[rel, at, :] = o[:, :L]
+            ps2[rel, at, :] = o[:, L:].astype(BF)
+            remote(ps2.at[rel, at], pr2.at[rel, at], send_sem.at[7], p2_sem.at[rel, hs], partner)
+
+    paired = set()
+
+    def pair_ready(rel, hs):
+        if (rel, hs) not in paired:
+            paired.add((rel, hs))
+            take(pr2.at[rel, pl.ds(hs * tall, tall)], p2_sem.at[rel, hs])
+
+    def stage_of(stage, hs):
+        for g in range(hs * (G // HS), (hs + 1) * (G // HS)):
             at = pl.ds(g * rows, rows)
             for way in range(2):
                 begin = half - hops(way, g)
                 if stage < begin:
                     continue
-                rel = rel_of[way]
+                rel = half - stage if way == 0 else (ny - half + stage) % ny
+                pair_ready(rel, hs)
                 s = own2[rel, at, :] + pr2[rel, at, :].astype(F32)
                 if stage > begin:
                     take(r2r.at[way, stage - 1, g], r2_sem.at[way, stage - 1, g])
@@ -392,8 +442,32 @@
                     r2_sem.at[way, stage, g],
                     side_of(way),
                 )
-    take(pr2.at[0], p2_sem.at[0])
-    for g in reversed(range(G)):
+
+    for g in range(G // HS):
+        catch(g, g % 2, half - 1)
+        if todo:
+            absorb(*todo.pop(0))
+    while todo:
+        absorb(*todo.pop(0))
+    absorb(half, 0)
+    activate(0)
+    for g in range(G // HS, G):
+        catch(g, g % 2, half - 1)
+    pending.append((ag.at[pl.ds(0, ny - 1)], send_sem.at[5]))
+    pending.append((ag.at[pl.ds(0, ny)], send_sem.at[6]))
+    ready("wd")
+    project(0)
+    absorb(half, 1)
+    activate(1)
+    stage_of(0, 0)
+    project(1)
+    pending.append((ps2, send_sem.at[7]))
+    stage_of(0, 1)
+    for stage in range(1, half):
+        for hs in range(HS):
+            stage_of(stage, hs)
+    for g in range(G):
+        pair_ready(0, g // (G // HS))
         at = pl.ds(g * rows, rows)
         s = own2[0, at, :] + pr2[0, at, :].astype(F32)
         for way in range(2):
@@ -406,7 +480,6 @@
                 continue
             tz, tx = sp_at(-pos[p][0], -pos[p][1])
             remote(out2.at[p], ret.at[me_s], send_sem.at[9], ret_sem.at[0], (tz, tx, y, c))
-
     pending.append((ps2.at[pl.ds(0, ny - 1)], send_sem.at[8]))
     pending.append((out2.at[pl.ds(0, ns - 1)], send_sem.at[9]))
     take(ret.at[pl.ds(0, ns - 1)], ret_sem.at[0])
@@ -436,6 +509,10 @@
     pending.append((out_hbm, loc_sem.at[5]))
     for ref, sem in pending:
         take(ref, sem)
+
+    @pl.when(me_s < ns - 1)
+    def _():
+        take(kv_ref, send_sem.at[0])
 
 
 def per_device(
@@ -476,6 +553,7 @@
         pltpu.VMEM((ny, hidden, 2 * L), BF),
         pltpu.VMEM((T, L), BF),
         pltpu.VMEM((2, HEAD_DIM, T), BF),
+        pltpu.VMEM((2, HEAD_DIM, T), BF),
         pltpu.VMEM((T, slots), BF),
         pltpu.VMEM((T, slots), BF),
         pltpu.VMEM((slots, T), BF),
@@ -506,12 +584,13 @@
         pltpu.SemaphoreType.DMA((ny,)),
         pltpu.SemaphoreType.DMA((G,)),
         pltpu.SemaphoreType.DMA((2, half, G)),
-        pltpu.SemaphoreType.DMA((ny,)),
-        pltpu.SemaphoreType.DMA((ny,)),
+        pltpu.SemaphoreType.DMA((ny + 1,)),
+        pltpu.SemaphoreType.DMA((ny, HS)),
         pltpu.SemaphoreType.DMA((2, half, G)),
         pltpu.SemaphoreType.DMA((1,)),
         pltpu.SemaphoreType.DMA((ny,)),
         pltpu.SemaphoreType.DMA((ny,)),
+        pltpu.SemaphoreType.REGULAR((max(1, (ns // 2).bit_length() - 1),)),
     ]
     return pl.pallas_call(
         functools.partial(layer, dims),

time: 87.2 us -> 89.3 us (1.024)
  Pallas kernels: 85.1 us -> 87.2 us
    pallas_call x1, Pallas kernels: 85.1 us -> 87.2 us  [per_device(): pl.pallas_call(functools.partial(layer, dims), out_shape=jax.ShapeDtypeSt...]
where the time goes in v3:
time: 89.3 us; the launch traced here: 89.1 us
  Pallas kernels  87.2 us (98%)
  local copies, waits for them, and re-layouts  1.88 us (2%)
    pallas_call x1, Pallas kernels, per_device(): pl.pallas_call(functools.partial(layer, dims), out_shape=jax.ShapeDtypeSt...  87.2 us
    unnamed x1, local copies, waits for them, and re-layouts  1.88 us

profile of v3, /device:TPU:1, one launch (start us, length us, event | category | flops | bytes accessed | tf_op | source)
XLA Modules:
  0.0 89.1 jit_solution(5241277550466482579)
XLA Ops:
  0.0 87.2 %layer.1 = bf16[128,2048]{1,0:T(8,128)(2,1)} custom-call(bf16[128,128]{1,0:T(8,128)(2,1)} %q_hbm.1, bf16[64,128]{1,0:T(8,128)(2,1)} %bitcast.5, bf16[64,128]{1,0:T(8,128)(2,1)} %bitcast.6, f32[2]{0:T(128)} %sink_ref.1, bf16[128,2048]{1,0:T(8,128)(2,1)} %wo_hbm.1, bf16[128,2048]{1,0:T(8,128)(2,1)} %res_hbm.1, f32[1,2048]{1,0:T(1,128)} %bitcast.7, ...), custom_call_target="tpu_custom_call" | custom-call | tf_op jit(solution)/shard_map/layer/pallas_call | solution.py:595
  87.2 1.9 %copy.14 = bf16[128,2048]{1,0:T(8,128)(2,1)} copy(bf16[128,2048]{1,0:T(8,128)(2,1)} %layer.1) | data formatting | bytes 1048576

commit v4 on v3

--- a/solution.py
+++ b/solution.py
@@ -144,25 +144,12 @@
     signal(barrier, along(1))
     signal(barrier, along(-1))
     signal(barrier, partner)
+    for d in range(1, nz):
+        signal(barrier, (*sp_at(d, 0), y, c))
+    for d in range(1, nx):
+        signal(barrier, (*sp_at(0, d), y, c))
     for rel in range(1, ny):
         signal(barrier, (z, x, at_y(rel), c))
-    shifts = [1 << i for i in range(know_sem.shape[0])]
-
-    def tell(i):
-        signal(know_sem.at[i], along(shifts[i]))
-        signal(know_sem.at[i], along(-shifts[i]))
-
-    def hear(i):
-        pl.semaphore_wait(know_sem.at[i], 2)
-        if i + 1 < len(shifts):
-            tell(i + 1)
-
-    heard = iter(range(len(shifts)))
-
-    def hear_next():
-        for i in heard:
-            hear(i)
-            return
 
     def lane_block(j):
         return pl.ds(pl.multiple_of(j * L, L), L)
@@ -237,8 +224,9 @@
 
     own_s = [masked(h, kv_ref[0], dist, lanes <= subs) for h in range(2)]
 
-    pl.semaphore_wait(barrier, ny + 2)
-    tell(0)
+    pl.semaphore_wait(barrier, nz + nx + ny)
+    for d in range(1, nz):
+        signal(know_sem, (*sp_at(d, 0), y, c))
 
     @pl.when(me_s < ns - 1)
     def _():
@@ -284,26 +272,21 @@
         ps1[rel] = o[:, L:].astype(BF)
         remote(ps1.at[rel], pr1.at[rel], send_sem.at[2], p1_sem.at[rel], partner)
     pending.append((ps1, send_sem.at[2]))
-    hear_next()
     for rel in rels[:-1]:
         take(pr1.at[rel], p1_sem.at[rel])
         r1s[rel] = (own1[rel] + pr1[rel].astype(F32)).astype(BF)
         remote(r1s.at[rel], r1r.at[rel], send_sem.at[3], r1_sem.at[rel], (z, x, at_y(rel), c))
     pending.append((r1s.at[pl.ds(0, ny - 1)], send_sem.at[3]))
-    hear_next()
     take(pr1.at[0], p1_sem.at[0])
     ready("res")
     total = res[...].astype(F32) + own1[0] + pr1[0].astype(F32)
-    for i, rel in enumerate(rels[-2::-1]):
+    for rel in rels[-2::-1]:
         take(r1r.at[rel], r1_sem.at[rel])
         total = total + r1r[rel].astype(F32)
-        if i == half:
-            hear_next()
     state = total.astype(BF)
     state_ref[...] = state
 
-    for i in heard:
-        hear(i)
+    pl.semaphore_wait(know_sem, nz - 1)
     disp[...] = dot(pick_ref[...], state).astype(BF).reshape(ns, cap, L)
     for p in range(1, ns):
         tz, tx = sp_at(*pos[p])
@@ -323,22 +306,30 @@
     def hops(way, g):
         return half if (way == 0) == (g % 2 == 0) else half - 1
 
-    def side_of(way):
-        return (z, x, at_y(1 if way == 0 else -1), c)
-
-    def pass_on(g, way, hop, j):
-        if hop < hops(way, g):
+    def side_of(way, d=1):
+        return (z, x, at_y(d if way == 0 else -d), c)
+
+    def far_group(g):
+        return g >= G // HS
+
+    def forward(g, way, dist, j, by):
+        if dist <= hops(way, g):
             remote(
                 ag.at[j, grp(g)],
                 ag.at[j, grp(g)],
                 send_sem.at[5],
-                agr_sem.at[way, hop, g],
-                side_of(way),
+                agr_sem.at[way, dist - 1, g],
+                side_of(way, by),
             )
 
     def across(g, j, rel):
-        at = ny if rel == half and g >= G // HS else rel
-        remote(ag.at[j, grp(g)], ag.at[j, grp(g)], send_sem.at[6], agd_sem.at[at], partner)
+        remote(
+            ag.at[j, grp(g)],
+            ag.at[j, grp(g)],
+            send_sem.at[6],
+            agd_sem.at[rel, g // (G // HS)],
+            partner,
+        )
 
     for g in range(G):
         if g == 0:
@@ -346,7 +337,9 @@
         else:
             take(ag.at[me_j, grp(g)], disp_sem.at[g])
         for way in range(2):
-            pass_on(g, way, 0, me_j)
+            if far_group(g):
+                forward(g, way, 2, me_j, 2)
+            forward(g, way, 1, me_j, 1)
         across(g, me_j, 0)
 
     ready("wg")
@@ -359,10 +352,7 @@
         yy = at_y(rel)
         other = 2 * yy + 1 - c
         part = pl.ds(hs * (ns // HS), ns // HS)
-        if rel == half:
-            take(ag.at[other, part], agd_sem.at[rel if hs == 0 else ny])
-        elif hs == 0:
-            take(ag.at[other], agd_sem.at[rel])
+        take(ag.at[other, part], agd_sem.at[rel, hs])
         cols = pl.ds(pl.multiple_of(yy * 2 * L, 2 * L), 2 * L)
         gain = gain_ref[:, cols]
         at = pl.ds(hs * tall, tall)
@@ -381,23 +371,35 @@
             acc_g[at, :] += dot(lhs, wg[cols, :])
             acc_u[at, :] += dot(lhs, wu[cols, :])
 
-    def catch(g, way, hop):
-        rel = ny - hop - 1 if way == 0 else hop + 1
+    def catch(g, way, dist):
+        rel = ny - dist if way == 0 else dist
         j = 2 * at_y(rel) + c
-        take(ag.at[j, grp(g)], agr_sem.at[way, hop, g])
-        pass_on(g, way, hop + 1, j)
+        take(ag.at[j, grp(g)], agr_sem.at[way, dist - 1, g])
+        if not far_group(g):
+            forward(g, way, dist + 1, j, 1)
+        elif dist == 2:
+            forward(g, way, 4, j, 2)
+            forward(g, way, 3, j, 1)
         across(g, j, rel)
 
-    todo = [(0, hs) for hs in range(HS)]
-    for hop in range(half - 1):
-        for g in range(G):
-            catch(g, 0, hop)
-            catch(g, 1, hop)
-            if g % 2 == 1 and todo:
-                absorb(*todo.pop(0))
-        while todo:
-            absorb(*todo.pop(0))
-        todo = [(rel, hs) for rel in (ny - hop - 1, hop + 1) for hs in range(HS)]
+    def catch_all(hs, dist):
+        for g in range(hs * (G // HS), (hs + 1) * (G // HS)):
+            for way in range(2):
+                if dist <= hops(way, g):
+                    catch(g, way, dist)
+
+    catch_all(0, 1)
+    catch_all(0, 2)
+    catch_all(1, 2)
+    catch_all(1, 1)
+    for rel in (0, 1, ny - 1):
+        for hs in range(HS):
+            absorb(rel, hs)
+    catch_all(0, 3)
+    for rel in (2, ny - 2):
+        for hs in range(HS):
+            absorb(rel, hs)
+    catch_all(1, 3)
 
     def activate(hs):
         at = pl.ds(hs * tall, tall)
@@ -421,58 +423,62 @@
             paired.add((rel, hs))
             take(pr2.at[rel, pl.ds(hs * tall, tall)], p2_sem.at[rel, hs])
 
-    def stage_of(stage, hs):
-        for g in range(hs * (G // HS), (hs + 1) * (G // HS)):
-            at = pl.ds(g * rows, rows)
+    def at_of(g):
+        return pl.ds(g * rows, rows)
+
+    def share(way, dist, g):
+        rel = dist if way == 0 else (ny - dist) % ny
+        pair_ready(rel, g // (G // HS))
+        return own2[rel, at_of(g), :] + pr2[rel, at_of(g), :].astype(F32)
+
+    def arrived(way, at, g):
+        take(r2r.at[way, at, g], r2_sem.at[way, at, g])
+        return r2r[way, at, g].astype(F32)
+
+    def send_sum(s, way, at, g, by):
+        r2s[way, at, g] = s.astype(BF)
+        remote(
+            r2s.at[way, at, g],
+            r2r.at[way, at, g],
+            send_sem.at[8],
+            r2_sem.at[way, at, g],
+            side_of(way, by),
+        )
+
+    def near_stage(stage):
+        for g in range(G // HS):
             for way in range(2):
                 begin = half - hops(way, g)
-                if stage < begin:
-                    continue
-                rel = half - stage if way == 0 else (ny - half + stage) % ny
-                pair_ready(rel, hs)
-                s = own2[rel, at, :] + pr2[rel, at, :].astype(F32)
-                if stage > begin:
-                    take(r2r.at[way, stage - 1, g], r2_sem.at[way, stage - 1, g])
-                    s = s + r2r[way, stage - 1, g].astype(F32)
-                r2s[way, stage, g] = s.astype(BF)
-                remote(
-                    r2s.at[way, stage, g],
-                    r2r.at[way, stage, g],
-                    send_sem.at[8],
-                    r2_sem.at[way, stage, g],
-                    side_of(way),
-                )
-
-    for g in range(G // HS):
-        catch(g, g % 2, half - 1)
-        if todo:
-            absorb(*todo.pop(0))
-    while todo:
-        absorb(*todo.pop(0))
-    absorb(half, 0)
-    activate(0)
-    for g in range(G // HS, G):
-        catch(g, g % 2, half - 1)
-    pending.append((ag.at[pl.ds(0, ny - 1)], send_sem.at[5]))
-    pending.append((ag.at[pl.ds(0, ny)], send_sem.at[6]))
-    ready("wd")
-    project(0)
-    absorb(half, 1)
-    activate(1)
-    stage_of(0, 0)
-    project(1)
-    pending.append((ps2, send_sem.at[7]))
-    stage_of(0, 1)
-    for stage in range(1, half):
-        for hs in range(HS):
-            stage_of(stage, hs)
-    for g in range(G):
-        pair_ready(0, g // (G // HS))
-        at = pl.ds(g * rows, rows)
-        s = own2[0, at, :] + pr2[0, at, :].astype(F32)
+                if stage >= begin:
+                    s = share(way, half - stage, g)
+                    if stage > begin:
+                        s = s + arrived(way, stage - 1, g)
+                    send_sum(s, way, stage, g, 1)
+
+    def far_start():
+        for g in range(G // HS, G):
+            for way in range(2):
+                if hops(way, g) >= 4:
+                    send_sum(share(way, 4, g), way, 1, g, 2)
+                send_sum(share(way, 3, g), way, 0, g, 1)
+        for g in range(G // HS, G):
+            for way in range(2):
+                send_sum(share(way, 1, g), way, 2, g, 1)
+
+    def far_middle():
+        for g in range(G // HS, G):
+            for way in range(2):
+                s = share(way, 2, g) + arrived(way, 0, g)
+                if hops(way, g) >= 4:
+                    s = s + arrived(way, 1, g)
+                send_sum(s, way, 3, g, 2)
+
+    def finish(g):
+        s = share(0, 0, g)
         for way in range(2):
-            take(r2r.at[way, half - 1, g], r2_sem.at[way, half - 1, g])
-            s = s + r2r[way, half - 1, g].astype(F32)
+            if far_group(g):
+                s = s + arrived(way, 2, g)
+            s = s + arrived(way, 3, g)
         out2[grp(g)] = s.astype(BF).reshape(per, cap, L)
         for p in reversed(range(g * per, (g + 1) * per)):
             if p == 0:
@@ -480,6 +486,31 @@
                 continue
             tz, tx = sp_at(-pos[p][0], -pos[p][1])
             remote(out2.at[p], ret.at[me_s], send_sem.at[9], ret_sem.at[0], (tz, tx, y, c))
+
+    for rel in (3, ny - 3):
+        absorb(rel, 0)
+    catch_all(0, 4)
+    for rel in (3, ny - 3):
+        absorb(rel, 1)
+    absorb(half, 0)
+    activate(0)
+    catch_all(1, 4)
+    pending.append((ag.at[pl.ds(0, ny - 1)], send_sem.at[5]))
+    pending.append((ag.at[pl.ds(0, ny)], send_sem.at[6]))
+    ready("wd")
+    project(0)
+    absorb(half, 1)
+    activate(1)
+    near_stage(0)
+    project(1)
+    pending.append((ps2, send_sem.at[7]))
+    far_start()
+    near_stage(1)
+    far_middle()
+    near_stage(2)
+    near_stage(3)
+    for g in reversed(range(G)):
+        finish(g)
     pending.append((ps2.at[pl.ds(0, ny - 1)], send_sem.at[8]))
     pending.append((out2.at[pl.ds(0, ns - 1)], send_sem.at[9]))
     take(ret.at[pl.ds(0, ns - 1)], ret_sem.at[0])
@@ -584,13 +615,13 @@
         pltpu.SemaphoreType.DMA((ny,)),
         pltpu.SemaphoreType.DMA((G,)),
         pltpu.SemaphoreType.DMA((2, half, G)),
-        pltpu.SemaphoreType.DMA((ny + 1,)),
+        pltpu.SemaphoreType.DMA((ny, HS)),
         pltpu.SemaphoreType.DMA((ny, HS)),
         pltpu.SemaphoreType.DMA((2, half, G)),
         pltpu.SemaphoreType.DMA((1,)),
         pltpu.SemaphoreType.DMA((ny,)),
         pltpu.SemaphoreType.DMA((ny,)),
-        pltpu.SemaphoreType.REGULAR((max(1, (ns // 2).bit_length() - 1),)),
+        pltpu.SemaphoreType.REGULAR,
     ]
     return pl.pallas_call(
         functools.partial(layer, dims),

time: 89.3 us -> 89.1 us (level)
  no operation moved by 1% of the time
where the time goes in v4:
time: 89.1 us; the launch traced here: 88.9 us
  Pallas kernels  87 us (98%)
  local copies, waits for them, and re-layouts  1.88 us (2%)
    pallas_call x1, Pallas kernels, per_device(): pl.pallas_call(functools.partial(layer, dims), out_shape=jax.ShapeDtypeSt...  87 us
    unnamed x1, local copies, waits for them, and re-layouts  1.88 us

profile of v4, /device:TPU:1, one launch (start us, length us, event | category | flops | bytes accessed | tf_op | source)
XLA Modules:
  0.0 88.9 jit_solution(12536389465664758136)
XLA Ops:
  0.0 87.0 %layer.1 = bf16[128,2048]{1,0:T(8,128)(2,1)} custom-call(bf16[128,128]{1,0:T(8,128)(2,1)} %q_hbm.1, bf16[64,128]{1,0:T(8,128)(2,1)} %bitcast.5, bf16[64,128]{1,0:T(8,128)(2,1)} %bitcast.6, f32[2]{0:T(128)} %sink_ref.1, bf16[128,2048]{1,0:T(8,128)(2,1)} %wo_hbm.1, bf16[128,2048]{1,0:T(8,128)(2,1)} %res_hbm.1, f32[1,2048]{1,0:T(1,128)} %bitcast.7, ...), custom_call_target="tpu_custom_call" | custom-call | tf_op jit(solution)/shard_map/layer/pallas_call | solution.py:626
  87.0 1.9 %copy.14 = bf16[128,2048]{1,0:T(8,128)(2,1)} copy(bf16[128,2048]{1,0:T(8,128)(2,1)} %layer.1) | data formatting | bytes 1048576
